TPU v7x, 32 devices: a whole 2x2x4 slice. The times are simulated.
32 devices in a mesh: sp: 8 (over z, x), tp: 4 (over y, core).
Axes of the slice: x: 2, y: 2, z: 4, core: 2. Of those that a mesh axis runs over, the one named last changes fastest.
Arguments:
- stream: bfloat16 [1024, 2048], P(('sp', 'tp')), may hold values from -2.5 to 2.5
- recurrence_input: bfloat16 [1024, 2, 1024], P('sp', None, 'tp'), may hold values from -6 to 6
- output_gate_input: bfloat16 [1024, 2, 1024], P('sp', None, 'tp'), may hold values from -6 to 6
- convolution_taps: bfloat16 [4, 2, 1024], P(None, None, 'tp'), may hold values from -4 to 4
- first_group_gates: bfloat16 [2, 16, 64, 64], P(None, 'tp'), may hold values from -0.75 to 0.75
- second_group_gates: bfloat16 [2, 8, 128, 128], P(None, 'tp'), may hold values from -0.5 to 0.5
- channel_decay: float32 [2, 1024], P(None, 'tp'), may hold values from 4.7 to 13.6
- position_log_extra: float32 [1024, 2, 1024], P('sp', None, 'tp'), may hold values from -1.4 to 0, as said below
- recurrence_output_weight: bfloat16 [2, 1024, 2048], P(None, 'tp'), may hold values from -0.125 to 0.125
- first_norm_gain: float32 [2048], replicated, may hold values from 0.1 to 1.9
- first_norm_bias: float32 [2048], replicated, may hold values from -1.75 to 1.75
- routed_expert_index: int32 [1024, 4], P('sp'), may hold values from 0 to 7, all different within a row; in each aligned block of 32 rows (0 to 31, 32 to 63, ...) at most 20 rows name the same one
- routed_expert_weight: float32 [1024, 4], P('sp'), may hold values from 0.25 to 1
- routed_gate_weight: bfloat16 [8, 2048, 512], P('sp', None, 'tp'), may hold values from -0.125 to 0.125
- routed_up_weight: bfloat16 [8, 2048, 512], P('sp', None, 'tp'), may hold values from -0.125 to 0.125
- routed_down_weight: bfloat16 [8, 512, 2048], P('sp', 'tp'), may hold values from -0.25 to 0.25
- shared_gate_weight: bfloat16 [2048, 512], replicated, may hold values from -0.125 to 0.125
- shared_up_weight: bfloat16 [2048, 512], replicated, may hold values from -0.125 to 0.125
- shared_down_weight: bfloat16 [512, 2048], replicated, may hold values from -0.25 to 0.25
- second_norm_gain: float32 [2048], replicated, may hold values from 0.1 to 1.9
- second_norm_bias: float32 [2048], replicated, may hold values from -1.75 to 1.75
Outputs:
- result: bfloat16 [1024, 2048], P(('sp', 'tp'))
Inputs may be any that keep to these rules, and one draw needn't show every extreme that they name: `routed_expert_index`: each row names 4 different experts. In each aligned block of 32 rows no expert is named more than 20 times, and in some block an expert is named exactly 20 times. `position_log_extra`: every entry is negative.
All inputs are finite; a program needn't handle non-finite values.
Results may differ from a plain program's by a relative error of at most 0.015.
Values may be sent and summed in bfloat16 or wider, within the bound.
A program may use at most 64 MiB of HBM per device.

v0:
```python
import functools

import jax
import jax.numpy as jnp
from jax import lax
from jax.experimental import pallas as pl
from jax.experimental.pallas import tpu as pltpu
from jax.sharding import PartitionSpec as P

RESIDUAL_SCALE = 8.0**0.25
NORM_EPSILON = 1e-05
LANES = 128
PIECES = 6
EARLY = 3
MESH = pl.DeviceIdType.MESH
F32 = jnp.float32
BF16 = jnp.bfloat16


def layer_norm(values, gain, bias):
    row_mean = jnp.mean(values, axis=-1, keepdims=True)
    spread = jnp.mean(jnp.square(values - row_mean), axis=-1, keepdims=True)
    return (values - row_mean) * lax.rsqrt(spread + NORM_EPSILON) * gain + bias


def expm1_negative(z):
    small = jnp.full_like(z, 1.0 / 40320.0)
    for n in (5040.0, 720.0, 120.0, 24.0, 6.0, 2.0, 1.0):
        small = small * z + 1.0 / n
    return jnp.where(z > -0.5, small * z, jnp.exp(z) - 1.0)


def softplus(y):
    u = jnp.exp(-jnp.abs(y))
    s = u / (2.0 + u)
    sq = s * s
    series = jnp.full_like(s, 1.0 / 17.0)
    for n in (15.0, 13.0, 11.0, 9.0, 7.0, 5.0, 3.0, 1.0):
        series = series * sq + 1.0 / n
    return jnp.maximum(y, 0.0) + 2.0 * s * series


def lane_blocks(maps_ref):
    kinds, heads, size, _ = maps_ref.shape
    per = LANES // size
    blocks = []
    for start in range(0, heads, per):
        sides = []
        for kind in range(kinds):
            if per == 1:
                sides.append(maps_ref[kind, start])
                continue
            tall = []
            for p in range(per):
                row = lax.broadcasted_iota(jnp.int32, (size, LANES), 0)
                col = lax.broadcasted_iota(jnp.int32, (size, LANES), 1)
                place = jnp.where(col == row + p * size, 1.0, 0.0).astype(BF16)
                tall.append(dot(maps_ref[kind, start + p], place))
            sides.append(jnp.concatenate(tall, axis=0).astype(BF16))
        blocks.append(jnp.concatenate(sides, axis=1))
    return blocks


def silu(v):
    return v * jax.nn.sigmoid(v)


def dot(a, b):
    return jnp.dot(a, b, preferred_element_type=F32)


def kernel(
    dims,
    stream, rec_in, gate_in, taps, small_maps, large_maps, channel_decay, extra, n1g, n1b, n2g, n2b,
    ids, wts,
    out_w_hbm, rg_hbm, ru_hbm, rd_hbm, sg_hbm, su_hbm, sd_hbm,
    result,
    padded, halo, carry_own, carry_in, wdense, w_in, out_w, w_gu, w_d, s_gu, s_d,
    part, part_in, rows, hid, y_part, x_in, z_out, z_in, moe,
    local_sem, halo_sem, carry_send, carry_recv, w_send, w_recv,
    wt_send, wt_recv, tp_send, tp_recv, ag_send, ag_recv, fw_send, fw_recv,
    xs_send, xs_recv, zs_send, zs_recv,
):
    sp_n, tp_n, inner = dims
    outer = sp_n // inner
    pairs = tp_n // 2
    sp, tp = lax.axis_index("sp"), lax.axis_index("tp")
    zi, xi = sp // inner, lax.rem(sp, inner)
    other_x = lax.rem(xi + 1, inner)
    x_peer = zi * inner + other_x
    half_c = lax.rem(tp, 2)
    yi = tp // 2
    mate = yi * 2 + (1 - half_c)
    length, chans = rec_in.shape
    quarter = stream.shape[0]
    fe = rg_hbm.shape[1]
    fs = sg_hbm.shape[1]

    def remote(src, dst, send, recv, where):
        return pltpu.make_async_remote_copy(
            src_ref=src, dst_ref=dst, send_sem=send, recv_sem=recv,
            device_id=where, device_id_type=MESH,
        )

    locals_ = [
        pltpu.make_async_copy(rg_hbm, w_gu.at[tp, :, pl.ds(0, fe)], local_sem.at[0]),
        pltpu.make_async_copy(ru_hbm, w_gu.at[tp, :, pl.ds(fe, fe)], local_sem.at[1]),
        pltpu.make_async_copy(rd_hbm, w_d.at[tp], local_sem.at[2]),
        pltpu.make_async_copy(out_w_hbm, out_w, local_sem.at[3]),
        pltpu.make_async_copy(sg_hbm, s_gu.at[:, pl.ds(0, fs)], local_sem.at[4]),
        pltpu.make_async_copy(su_hbm, s_gu.at[:, pl.ds(fs, fs)], local_sem.at[5]),
        pltpu.make_async_copy(sd_hbm, s_d, local_sem.at[6]),
    ]

    halo_copy = remote(
        rec_in.at[pl.ds(length - 16, 16)], halo, halo_sem.at[0], halo_sem.at[1],
        (lax.rem(sp + 1, sp_n), tp),
    )
    halo_copy.start()

    depth = rg_hbm.shape[0] // 2
    fe_half = fe // 2

    def weight_src(piece):
        kind, part_id = piece // 2, piece % 2
        if kind == 2:
            return rd_hbm.at[pl.ds(part_id * fe_half, fe_half)]
        return (rg_hbm, ru_hbm)[kind].at[pl.ds(part_id * depth, depth)]

    def weight_dst(slot, piece):
        kind, part_id = piece // 2, piece % 2
        if kind == 2:
            return w_d.at[slot, pl.ds(part_id * fe_half, fe_half)]
        return w_gu.at[slot, pl.ds(part_id * depth, depth), pl.ds(kind * fe, fe)]

    def weight_out(kind, step):
        return remote(
            weight_src(kind), weight_dst(tp, kind),
            wt_send.at[kind, step], wt_recv.at[kind, tp],
            (sp, lax.rem(yi + step, pairs) * 2 + half_c),
        )

    def weight_mate(kind, slot, step):
        src = weight_src(kind) if step == 0 else weight_dst(slot, kind)
        return remote(
            src, weight_dst(slot, kind),
            wt_send.at[kind, pairs + step], wt_recv.at[kind, slot], (sp, mate),
        )

    def pair_slot(step):
        return lax.rem(yi + step, pairs) * 2 + half_c

    for piece in range(EARLY):
        for step in range(1, pairs):
            weight_out(piece, step).start()
    locals_[3].start()
    for piece in range(PIECES):
        weight_mate(piece, tp, 0).start()
    for i in range(3):
        locals_[i].start()
    for i in (4, 5, 6):
        locals_[i].start()

    expert = lax.broadcasted_iota(jnp.int32, (wdense.shape[0], length), 0)
    table = jnp.zeros((wdense.shape[0], length), F32)
    for k in range(ids.shape[0]):
        table = table + jnp.where(expert == ids[k : k + 1], wts[k : k + 1], 0.0)
    wdense[...] = table
    w_in[sp] = table

    def w_out(step):
        return remote(
            wdense, w_in.at[sp], w_send.at[step], w_recv.at[sp], (lax.rem(sp + step, sp_n), tp)
        )

    @pl.loop(1, sp_n)
    def _(step):
        w_out(step).start()

    small_blocks, large_blocks = lane_blocks(small_maps), lane_blocks(large_maps)
    rate_rows = -8.0 * softplus(-channel_decay[...])
    rate = jnp.concatenate([rate_rows[0:1], rate_rows[1:2]], axis=1)
    tap_rows = [
        jnp.concatenate([taps[k, 0:1], taps[k, 1:2]], axis=1).astype(F32)
        for k in range(taps.shape[0])
    ]

    padded[pl.ds(8, length)] = rec_in[...].astype(F32)
    halo_copy.wait()
    border = halo[...].astype(F32)[8:16]
    padded[pl.ds(0, 8)] = jnp.where(sp > 0, border, jnp.zeros_like(border))
    tap_n = taps.shape[0]
    summed = tap_rows[0] * padded[pl.ds(8 - tap_n + 1, length)]
    for k in range(1, tap_n):
        summed = summed + tap_rows[k] * padded[pl.ds(8 - tap_n + 1 + k, length)]
    conv = summed.astype(BF16)
    outs = [
        dot(conv[:, i * LANES : (i + 1) * LANES], maps)
        for i, maps in enumerate(small_blocks + large_blocks)
    ]
    recur = jax.nn.sigmoid(jnp.concatenate([o[:, :LANES] for o in outs], axis=1))
    inp = jax.nn.sigmoid(jnp.concatenate([o[:, LANES:] for o in outs], axis=1))
    log_decay = recur * rate + extra[...]
    decay = jnp.exp(log_decay)
    state = jnp.sqrt(-expm1_negative(2.0 * log_decay)) * inp * conv.astype(F32)
    row_id = lax.broadcasted_iota(jnp.int32, (length, chans), 0)
    shift = 1
    while shift < length:
        live = row_id >= shift
        before_a = jnp.where(live, pltpu.roll(decay, shift, 0), 1.0)
        before_b = jnp.where(live, pltpu.roll(state, shift, 0), 0.0)
        state = decay * before_b + state
        decay = decay * before_a
        shift *= 2
    carry_own[...] = jnp.concatenate(
        [decay[length - 1 :], state[length - 1 :], jnp.zeros((6, chans), F32)], axis=0
    )

    def carry_out(step):
        return remote(
            carry_own, carry_in.at[sp], carry_send.at[step], carry_recv.at[sp],
            (lax.rem(sp + step, sp_n), tp),
        )

    def carry_arrival(who):
        return remote(
            carry_own, carry_in.at[who], carry_send.at[0], carry_recv.at[who], (sp, tp)
        )

    @pl.loop(1, sp_n)
    def _(step):
        carry_out(step).start()

    gi = gate_in[...].astype(F32)
    gelu = 0.5 * gi * (1.0 + jnp.tanh(0.7978845608028654 * (gi + 0.044715 * gi * gi * gi)))

    @pl.loop(1, sp_n)
    def _(step):
        carry_arrival(lax.rem(sp + step, sp_n)).wait_recv()

    carry_in[sp] = carry_own[...]

    def fold(who, incoming):
        link = carry_in[who]
        return jnp.where(who < sp, link[0:1] * incoming + link[1:2], incoming)

    incoming = lax.fori_loop(0, sp_n, fold, jnp.zeros((1, chans), F32))
    branch = (gelu * (state + decay * incoming)).astype(BF16)
    locals_[3].wait()
    part[...] = dot(branch, out_w[...]).astype(BF16).reshape(part.shape)

    def part_out(step):
        to = lax.rem(tp + step, tp_n)
        return remote(
            part.at[to], part_in.at[tp], tp_send.at[step], tp_recv.at[tp], (sp, to)
        )

    def part_arrival(who):
        return remote(part.at[who], part_in.at[who], tp_send.at[0], tp_recv.at[who], (sp, tp))

    for step in range(1, tp_n):
        part_out(step).start()
    for piece in range(EARLY, PIECES):
        for step in range(1, pairs):
            weight_out(piece, step).start()
    mixed = part[tp].astype(F32)
    for step in range(1, tp_n):
        who = lax.rem(tp + step, tp_n)
        part_arrival(who).wait_recv()
        mixed = mixed + part_in[who].astype(F32)
    normed = layer_norm(
        RESIDUAL_SCALE * stream[...].astype(F32) + mixed, n1g[...], n1b[...]
    ).astype(BF16)
    rows[sp] = normed

    def ag_out(step):
        return remote(
            rows.at[sp], rows.at[sp], ag_send.at[step], ag_recv.at[sp],
            (lax.rem(zi + step, outer) * inner + xi, tp),
        )

    def ag_arrival(who):
        return remote(rows.at[who], rows.at[who], ag_send.at[0], ag_recv.at[who], (sp, tp))

    def forward(who):
        return remote(
            rows.at[who], rows.at[who], fw_send.at[who], ag_recv.at[who], (x_peer, tp)
        )

    @pl.loop(1, outer)
    def _(step):
        ag_out(step).start()

    forward(sp).start()

    def weight_arrival(kind, slot):
        return remote(
            weight_dst(slot, kind), weight_dst(slot, kind),
            wt_send.at[kind, 0], wt_recv.at[kind, slot], (sp, mate),
        )

    def relay(piece):
        for step in range(1, pairs):
            weight_arrival(piece, pair_slot(step)).wait_recv()
            weight_mate(piece, pair_slot(step), step).start()

    for piece in range(EARLY):
        relay(piece)

    locals_[4].wait()
    locals_[5].wait()
    locals_[6].wait()
    up = dot(normed, s_gu[...])
    s_hid = (silu(up[:, :fs]) * up[:, fs:]).astype(BF16)
    moe[...] = dot(s_hid, s_d[...]) + RESIDUAL_SCALE * normed.astype(F32)

    @pl.loop(1, sp_n)
    def _(step):
        who = lax.rem(sp + step, sp_n)
        remote(wdense, w_in.at[who], w_send.at[0], w_recv.at[who], (sp, tp)).wait_recv()

    for i in range(3):
        locals_[i].wait()

    @pl.loop(1, outer)
    def _(step):
        mine = lax.rem(zi + step, outer) * inner + xi
        ag_arrival(mine).wait_recv()
        forward(mine).start()

    for piece in range(EARLY, PIECES):
        relay(piece)

    @pl.loop(0, outer)
    def _(step):
        ag_arrival(step * inner + other_x).wait_recv()

    for piece in range(PIECES):
        for step in range(pairs):
            weight_arrival(piece, lax.rem(yi + step, pairs) * 2 + 1 - half_c).wait_recv()

    width = stream.shape[1]
    grp = inner * quarter
    batch = min(sp_n, 8)

    @pl.loop(0, sp_n // batch)
    def _(i):
        block = rows[pl.ds(i * batch, batch)].reshape(batch * quarter, width)
        for t in range(tp_n):
            gu = dot(block, w_gu[t])
            act = (silu(gu[:, :fe]) * gu[:, fe:]).astype(BF16)
            hid[pl.ds(i * batch, batch), :, t * fe : (t + 1) * fe] = act.reshape(
                batch, quarter, fe
            )

    def x_out(zj):
        return remote(
            y_part.at[zj * inner + other_x], x_in.at[zj], xs_send.at[zj], xs_recv.at[zj],
            (x_peer, tp),
        )

    own_rows = lax.broadcasted_iota(jnp.int32, (quarter, length), 0) + tp * quarter
    pick = lax.broadcasted_iota(jnp.int32, (quarter, length), 1) == own_rows

    @pl.loop(1, outer + 1)
    def _(step):
        zj = lax.rem(zi + step, outer)
        block = hid[pl.ds(zj * inner, inner)].reshape(grp, tp_n * fe)
        value = dot(block, w_d[...].reshape(tp_n * fe, width))
        for j in range(inner):
            line = w_in[zj * inner + j, pl.ds(sp, 1)]
            weight = jnp.sum(jnp.where(pick, line, 0.0), axis=1, keepdims=True)
            y_part[zj * inner + j] = (
                weight * value[j * quarter : (j + 1) * quarter]
            ).astype(BF16)
        x_out(zj).start()

    def z_send(step):
        zj = lax.rem(zi + step, outer)
        return remote(
            z_out.at[zj], z_in.at[zi], zs_send.at[step], zs_recv.at[zi], (zj * inner + xi, tp)
        )

    @pl.loop(1, outer)
    def _(step):
        zj = lax.rem(zi + step, outer)
        x_out(zj).wait_recv()
        both = y_part[zj * inner + xi].astype(F32) + x_in[zj].astype(F32)
        z_out[zj] = both.astype(BF16)
        z_send(step).start()

    x_out(zi).wait_recv()
    moe[...] += y_part[sp].astype(F32) + x_in[zi].astype(F32)

    @pl.loop(1, outer)
    def _(step):
        zj = lax.rem(zi + step, outer)
        remote(z_out.at[zj], z_in.at[zj], zs_send.at[0], zs_recv.at[zj], (sp, tp)).wait_recv()
        moe[...] += z_in[zj].astype(F32)

    result[...] = layer_norm(moe[...], n2g[...], n2b[...]).astype(BF16)

    for kind in range(PIECES):
        for step in range(1, pairs):
            weight_out(kind, step).wait_send()
            weight_mate(kind, pair_slot(step), step).wait_send()
        weight_mate(kind, tp, 0).wait_send()
    for step in range(1, tp_n):
        part_out(step).wait_send()

    @pl.loop(1, sp_n)
    def _(step):
        w_out(step).wait_send()
        carry_out(step).wait_send()

    @pl.loop(1, outer)
    def _(step):
        ag_out(step).wait_send()
        z_send(step).wait_send()

    @pl.loop(0, outer)
    def _(step):
        forward(step * inner + xi).wait_send()
        x_out(step).wait_send()


def shards(
    dims,
    stream,
    recurrence_input,
    output_gate_input,
    convolution_taps,
    first_group_gates,
    second_group_gates,
    channel_decay,
    position_log_extra,
    recurrence_output_weight,
    first_norm_gain,
    first_norm_bias,
    routed_expert_index,
    routed_expert_weight,
    routed_gate_weight,
    routed_up_weight,
    routed_down_weight,
    shared_gate_weight,
    shared_up_weight,
    shared_down_weight,
    second_norm_gain,
    second_norm_bias,
):
    sp_n, tp_n, inner = dims
    outer = sp_n // inner
    length = recurrence_input.shape[0]
    chans = 2 * recurrence_input.shape[2]
    quarter, width = stream.shape
    fe = routed_gate_weight.shape[2]
    fs = shared_gate_weight.shape[1]
    flat = lambda a: a.reshape(a.shape[0], chans)
    vec = lambda a: a.reshape(1, width)
    vmem = pl.BlockSpec(memory_space=pltpu.VMEM)
    hbm = pl.BlockSpec(memory_space=pl.ANY)
    dma = pltpu.SemaphoreType.DMA
    block = (quarter, width)
    pairs = tp_n // 2
    return pl.pallas_call(
        functools.partial(kernel, dims),
        out_shape=jax.ShapeDtypeStruct(block, BF16),
        in_specs=[vmem] * 14 + [hbm] * 7,
        out_specs=vmem,
        scratch_shapes=[
            pltpu.VMEM((length + 8, chans), F32),
            pltpu.VMEM((16, chans), BF16),
            pltpu.VMEM((8, chans), F32),
            pltpu.VMEM((sp_n, 8, chans), F32),
            pltpu.VMEM((sp_n, length), F32),
            pltpu.VMEM((sp_n, sp_n, length), F32),
            pltpu.VMEM((chans, width), BF16),
            pltpu.VMEM((tp_n, width, 2 * fe), BF16),
            pltpu.VMEM((tp_n, fe, width), BF16),
            pltpu.VMEM((width, 2 * fs), BF16),
            pltpu.VMEM((fs, width), BF16),
            pltpu.VMEM((tp_n,) + block, BF16),
            pltpu.VMEM((tp_n,) + block, BF16),
            pltpu.VMEM((sp_n,) + block, BF16),
            pltpu.VMEM((sp_n, quarter, tp_n * fe), BF16),
            pltpu.VMEM((sp_n,) + block, BF16),
            pltpu.VMEM((outer,) + block, BF16),
            pltpu.VMEM((outer,) + block, BF16),
            pltpu.VMEM((outer,) + block, BF16),
            pltpu.VMEM(block, F32),
            dma((8,)),
            dma((2,)),
            dma((sp_n,)),
            dma((sp_n,)),
            dma((sp_n,)),
            dma((sp_n,)),
            dma((PIECES, 2 * pairs)),
            dma((PIECES, tp_n)),
            dma((tp_n,)),
            dma((tp_n,)),
            dma((outer,)),
            dma((sp_n,)),
            dma((sp_n,)),
            dma((1,)),
            dma((outer,)),
            dma((outer,)),
            dma((outer,)),
            dma((outer,)),
        ],
        compiler_params=pltpu.CompilerParams(
            has_side_effects=True, vmem_limit_bytes=60 * 2**20
        ),
    )(
        stream,
        flat(recurrence_input),
        flat(output_gate_input),
        convolution_taps,
        first_group_gates,
        second_group_gates,
        channel_decay,
        flat(position_log_extra),
        vec(first_norm_gain),
        vec(first_norm_bias),
        vec(second_norm_gain),
        vec(second_norm_bias),
        routed_expert_index.T,
        routed_expert_weight.T,
        recurrence_output_weight.reshape(chans, width),
        routed_gate_weight.reshape(width, fe),
        routed_up_weight.reshape(width, fe),
        routed_down_weight.reshape(fe, width),
        shared_gate_weight,
        shared_up_weight,
        shared_down_weight,
    )


def solution(mesh):
    in_specs = (
        P(("sp", "tp"), None),
        P("sp", None, "tp"),
        P("sp", None, "tp"),
        P(None, None, "tp"),
        P(None, "tp", None, None),
        P(None, "tp", None, None),
        P(None, "tp"),
        P("sp", None, "tp"),
        P(None, "tp", None),
        P(),
        P(),
        P("sp", None),
        P("sp", None),
        P("sp", None, "tp"),
        P("sp", None, "tp"),
        P("sp", "tp", None),
        P(),
        P(),
        P(),
        P(),
        P(),
    )
    dims = (mesh.shape["sp"], mesh.shape["tp"], 2)
    return jax.shard_map(
        functools.partial(shards, dims),
        mesh=mesh,
        in_specs=in_specs,
        out_specs=P(("sp", "tp"), None),
        check_vma=False,
    )
```

profile of v0, /device:TPU:0, one launch (start us, length us, event | category | flops | bytes accessed | tf_op | source)
XLA Modules:
  0.0 83.5 jit_solution(12635204757703253968)
XLA Ops:
  0.0 1.6 %copy.22 = bf16[16,8,2,256]{3,1,2,0:T(8,128)(2,1)} copy(bf16[16,8,2,256]{3,2,1,0:T(2,128)(2,1)} %bitcast.24) | data formatting | bytes 262144
  1.6 1.6 %copy.23 = bf16[16,8,2,256]{3,1,2,0:T(8,128)(2,1)} copy(bf16[16,8,2,256]{3,2,1,0:T(2,128)(2,1)} %bitcast.25) | data formatting | bytes 262144
  3.2 1.7 %copy.24 = f32[16,8,2,256]{3,1,2,0:T(8,128)} copy(f32[16,8,2,256]{3,2,1,0:T(2,128)} %bitcast.23) | data formatting | bytes 524288
  4.8 77.1 %shard_map.199 = bf16[32,2048]{1,0:T(8,128)(2,1)} custom-call(bf16[32,2048]{1,0:T(8,128)(2,1)} %stream.1, bf16[128,512]{1,0:T(8,128)(2,1)} %bitcast.21, bf16[128,512]{1,0:T(8,128)(2,1)} %bitcast.22, bf16[4,2,256]{2,1,0:T(2,128)(2,1)} %taps.1, bf16[2,4,64,64]{3,2,1,0:T(8,128)(2,1)} %small_maps.1, bf16[2,2,128,128]{3,2,1,0:T(8,128)(2,1)} %large_maps.1, ...), custom_call_target="tpu_custom_call" | custom-call | tf_op jit(solution)/shard_map/pallas_call | solution.py:465
  81.9 1.6 %copy.26 = bf16[32,2048]{1,0:T(8,128)(2,1)} copy(bf16[32,2048]{1,0:T(8,128)(2,1)} %shard_map.199) | data formatting | bytes 262144
where the time goes:
time: 83.7 us; the launch traced here: 83.5 us
  Pallas kernels  77.1 us (92%)
  local copies, waits for them, and re-layouts  6.38 us (8%)
    pallas_call x1, Pallas kernels, shards(): pl.pallas_call(functools.partial(kernel, dims), out_shape=jax.ShapeDtypeS...  77.1 us
    unnamed x4, local copies, waits for them, and re-layouts  6.38 us

commit v1 on v0

--- a/solution.py
+++ b/solution.py
@@ -71,10 +71,12 @@
 
 def kernel(
     dims,
-    stream, rec_in, gate_in, taps, small_maps, large_maps, channel_decay, extra, n1g, n1b, n2g, n2b,
-    ids, wts,
+    stream_hbm, rec_hbm, gate_hbm, taps_hbm, small_hbm, large_hbm, decay_hbm, extra_hbm,
+    n1g_hbm, n1b_hbm, n2g_hbm, n2b_hbm, ids_hbm, wts_hbm,
     out_w_hbm, rg_hbm, ru_hbm, rd_hbm, sg_hbm, su_hbm, sd_hbm,
     result,
+    stream, rec_in, gate_in, taps, small_maps, large_maps, channel_decay, extra, n1g, n1b, n2g, n2b,
+    ids, wts, in_sem,
     padded, halo, carry_own, carry_in, wdense, w_in, out_w, w_gu, w_d, s_gu, s_d,
     part, part_in, rows, hid, y_part, x_in, z_out, z_in, moe,
     local_sem, halo_sem, carry_send, carry_recv, w_send, w_recv,
@@ -91,10 +93,38 @@
     half_c = lax.rem(tp, 2)
     yi = tp // 2
     mate = yi * 2 + (1 - half_c)
-    length, chans = rec_in.shape
+    length = rec_in.shape[0]
+    chans = rec_in.shape[1] * rec_in.shape[2]
     quarter = stream.shape[0]
     fe = rg_hbm.shape[1]
     fs = sg_hbm.shape[1]
+
+    loads = [
+        pltpu.make_async_copy(src, dst, in_sem.at[i])
+        for i, (src, dst) in enumerate([
+            (rec_hbm, rec_in), (small_hbm, small_maps), (large_hbm, large_maps), (taps_hbm, taps),
+            (decay_hbm, channel_decay), (extra_hbm, extra), (gate_hbm, gate_in), (ids_hbm, ids),
+            (wts_hbm, wts), (stream_hbm, stream), (n1g_hbm, n1g), (n1b_hbm, n1b), (n2g_hbm, n2g),
+            (n2b_hbm, n2b),
+        ])
+    ]
+    for load in loads:
+        load.start()
+    barrier = pltpu.get_barrier_semaphore()
+
+    @pl.loop(1, sp_n)
+    def _(step):
+        pl.semaphore_signal(
+            barrier, inc=1, device_id=(lax.rem(sp + step, sp_n), tp), device_id_type=MESH
+        )
+
+    for step in range(1, tp_n):
+        pl.semaphore_signal(
+            barrier, inc=1, device_id=(sp, lax.rem(tp + step, tp_n)), device_id_type=MESH
+        )
+    for load in loads:
+        load.wait()
+    pl.semaphore_wait(barrier, sp_n - 1 + tp_n - 1)
 
     def remote(src, dst, send, recv, where):
         return pltpu.make_async_remote_copy(
@@ -113,10 +143,13 @@
     ]
 
     halo_copy = remote(
-        rec_in.at[pl.ds(length - 16, 16)], halo, halo_sem.at[0], halo_sem.at[1],
+        rec_in.at[pl.ds(length - 8, 8)], halo, halo_sem.at[0], halo_sem.at[1],
         (lax.rem(sp + 1, sp_n), tp),
     )
-    halo_copy.start()
+
+    @pl.when(sp + 1 < sp_n)
+    def _():
+        halo_copy.start()
 
     depth = rg_hbm.shape[0] // 2
     fe_half = fe // 2
@@ -185,10 +218,17 @@
         for k in range(taps.shape[0])
     ]
 
-    padded[pl.ds(8, length)] = rec_in[...].astype(F32)
-    halo_copy.wait()
-    border = halo[...].astype(F32)[8:16]
-    padded[pl.ds(0, 8)] = jnp.where(sp > 0, border, jnp.zeros_like(border))
+    padded[pl.ds(8, length)] = rec_in[...].astype(F32).reshape(length, chans)
+
+    @pl.when(sp == 0)
+    def _():
+        padded[pl.ds(0, 8)] = jnp.zeros((8, chans), F32)
+
+    @pl.when(sp > 0)
+    def _():
+        halo_copy.wait_recv()
+        padded[pl.ds(0, 8)] = halo[...].astype(F32).reshape(8, chans)
+
     tap_n = taps.shape[0]
     summed = tap_rows[0] * padded[pl.ds(8 - tap_n + 1, length)]
     for k in range(1, tap_n):
@@ -200,7 +240,7 @@
     ]
     recur = jax.nn.sigmoid(jnp.concatenate([o[:, :LANES] for o in outs], axis=1))
     inp = jax.nn.sigmoid(jnp.concatenate([o[:, LANES:] for o in outs], axis=1))
-    log_decay = recur * rate + extra[...]
+    log_decay = recur * rate + extra[...].reshape(length, chans)
     decay = jnp.exp(log_decay)
     state = jnp.sqrt(-expm1_negative(2.0 * log_decay)) * inp * conv.astype(F32)
     row_id = lax.broadcasted_iota(jnp.int32, (length, chans), 0)
@@ -213,7 +253,7 @@
         decay = decay * before_a
         shift *= 2
     carry_own[...] = jnp.concatenate(
-        [decay[length - 1 :], state[length - 1 :], jnp.zeros((6, chans), F32)], axis=0
+        [decay[length - 1 :], state[length - 1 :]], axis=0
     )
 
     def carry_out(step):
@@ -229,22 +269,19 @@
 
     @pl.loop(1, sp_n)
     def _(step):
-        carry_out(step).start()
-
-    gi = gate_in[...].astype(F32)
+        @pl.when(sp + step < sp_n)
+        def _():
+            carry_out(step).start()
+
+    gi = gate_in[...].astype(F32).reshape(length, chans)
     gelu = 0.5 * gi * (1.0 + jnp.tanh(0.7978845608028654 * (gi + 0.044715 * gi * gi * gi)))
 
-    @pl.loop(1, sp_n)
-    def _(step):
-        carry_arrival(lax.rem(sp + step, sp_n)).wait_recv()
-
-    carry_in[sp] = carry_own[...]
-
     def fold(who, incoming):
+        carry_arrival(who).wait_recv()
         link = carry_in[who]
-        return jnp.where(who < sp, link[0:1] * incoming + link[1:2], incoming)
-
-    incoming = lax.fori_loop(0, sp_n, fold, jnp.zeros((1, chans), F32))
+        return link[0:1] * incoming + link[1:2]
+
+    incoming = lax.fori_loop(0, sp, fold, jnp.zeros((1, chans), F32))
     branch = (gelu * (state + decay * incoming)).astype(BF16)
     locals_[3].wait()
     part[...] = dot(branch, out_w[...]).astype(BF16).reshape(part.shape)
@@ -411,7 +448,14 @@
     @pl.loop(1, sp_n)
     def _(step):
         w_out(step).wait_send()
-        carry_out(step).wait_send()
+
+        @pl.when(sp + step < sp_n)
+        def _():
+            carry_out(step).wait_send()
+
+    @pl.when(sp + 1 < sp_n)
+    def _():
+        halo_copy.wait_send()
 
     @pl.loop(1, outer)
     def _(step):
@@ -455,23 +499,52 @@
     quarter, width = stream.shape
     fe = routed_gate_weight.shape[2]
     fs = shared_gate_weight.shape[1]
-    flat = lambda a: a.reshape(a.shape[0], chans)
     vec = lambda a: a.reshape(1, width)
     vmem = pl.BlockSpec(memory_space=pltpu.VMEM)
-    hbm = pl.BlockSpec(memory_space=pl.ANY)
+    hbm = pl.BlockSpec(memory_space=pltpu.HBM)
     dma = pltpu.SemaphoreType.DMA
     block = (quarter, width)
     pairs = tp_n // 2
+    operands = (
+        stream,
+        recurrence_input,
+        output_gate_input,
+        convolution_taps,
+        first_group_gates,
+        second_group_gates,
+        channel_decay,
+        position_log_extra,
+        vec(first_norm_gain),
+        vec(first_norm_bias),
+        vec(second_norm_gain),
+        vec(second_norm_bias),
+        routed_expert_index.T,
+        routed_expert_weight.T,
+    )
+    weights = (
+        recurrence_output_weight.reshape(chans, width),
+        routed_gate_weight.reshape(width, fe),
+        routed_up_weight.reshape(width, fe),
+        routed_down_weight.reshape(fe, width),
+        shared_gate_weight,
+        shared_up_weight,
+        shared_down_weight,
+    )
+    limit = (28 + sp_n // 2) * 2**20
+    operands = tuple(pltpu.with_memory_space_constraint(a, pltpu.HBM) for a in operands)
+    weights = tuple(pltpu.with_memory_space_constraint(a, pltpu.HBM) for a in weights)
     return pl.pallas_call(
         functools.partial(kernel, dims),
         out_shape=jax.ShapeDtypeStruct(block, BF16),
-        in_specs=[vmem] * 14 + [hbm] * 7,
+        in_specs=[hbm] * (len(operands) + len(weights)),
         out_specs=vmem,
         scratch_shapes=[
+            *(pltpu.VMEM(a.shape, a.dtype) for a in operands),
+            dma((len(operands),)),
             pltpu.VMEM((length + 8, chans), F32),
-            pltpu.VMEM((16, chans), BF16),
-            pltpu.VMEM((8, chans), F32),
-            pltpu.VMEM((sp_n, 8, chans), F32),
+            pltpu.VMEM((8,) + recurrence_input.shape[1:], BF16),
+            pltpu.VMEM((2, chans), F32),
+            pltpu.VMEM((sp_n, 2, chans), F32),
             pltpu.VMEM((sp_n, length), F32),
             pltpu.VMEM((sp_n, sp_n, length), F32),
             pltpu.VMEM((chans, width), BF16),
@@ -508,31 +581,9 @@
             dma((outer,)),
         ],
         compiler_params=pltpu.CompilerParams(
-            has_side_effects=True, vmem_limit_bytes=60 * 2**20
+            has_side_effects=True, collective_id=0, vmem_limit_bytes=limit
         ),
-    )(
-        stream,
-        flat(recurrence_input),
-        flat(output_gate_input),
-        convolution_taps,
-        first_group_gates,
-        second_group_gates,
-        channel_decay,
-        flat(position_log_extra),
-        vec(first_norm_gain),
-        vec(first_norm_bias),
-        vec(second_norm_gain),
-        vec(second_norm_bias),
-        routed_expert_index.T,
-        routed_expert_weight.T,
-        recurrence_output_weight.reshape(chans, width),
-        routed_gate_weight.reshape(width, fe),
-        routed_up_weight.reshape(width, fe),
-        routed_down_weight.reshape(fe, width),
-        shared_gate_weight,
-        shared_up_weight,
-        shared_down_weight,
-    )
+    )(*operands, *weights)
 
 
 def solution(mesh):

time: 83.7 us -> 72.4 us (0.86)
  local copies, waits for them, and re-layouts: 6.38 us -> 0.66 us
  Pallas kernels: 77.1 us -> 71.6 us
    unnamed x4 -> x1, local copies, waits for them, and re-layouts: 6.38 us -> 0.66 us
    pallas_call x1, Pallas kernels: 77.1 us -> 71.6 us  [shards(): pl.pallas_call(functools.partial(kernel, dims), out_shape=jax.ShapeDtypeS...]
where the time goes in v1:
time: 72.4 us; the launch traced here: 72.2 us
  Pallas kernels  71.6 us (99%)
    pallas_call x1, Pallas kernels, shards(): pl.pallas_call(functools.partial(kernel, dims), out_shape=jax.ShapeDtypeS...  71.6 us

profile of v1, /device:TPU:0, one launch (start us, length us, event | category | flops | bytes accessed | tf_op | source)
XLA Modules:
  0.0 72.2 jit_solution(9759303130446915130)
XLA Ops:
  0.0 71.6 %shard_map.199 = bf16[32,2048]{1,0:T(8,128)(2,1)S(1)} custom-call(bf16[32,2048]{1,0:T(8,128)(2,1)} %stream_hbm.1, bf16[128,2,256]{2,1,0:T(2,128)(2,1)} %rec_hbm.1, bf16[128,2,256]{2,1,0:T(2,128)(2,1)} %gate_hbm.1, bf16[4,2,256]{2,1,0:T(2,128)(2,1)} %taps_hbm.1, bf16[2,4,64,64]{3,2,1,0:T(8,128)(2,1)} %small_hbm.1, bf16[2,2,128,128]{3,2,1,0:T(8,128)(2,1)} %large_hbm.1, ...), custom_call_target="tpu_custom_call" | custom-call | tf_op jit(solution)/shard_map/pallas_call | solution.py:536
  71.6 0.7 copy.23

commit v2 on v1

--- a/solution.py
+++ b/solution.py
@@ -10,8 +10,10 @@
 RESIDUAL_SCALE = 8.0**0.25
 NORM_EPSILON = 1e-05
 LANES = 128
-PIECES = 6
-EARLY = 3
+ROW_CUTS = 4
+COLUMN_CUTS = 4
+EARLY = 4
+SPLITS = 2
 MESH = pl.DeviceIdType.MESH
 F32 = jnp.float32
 BF16 = jnp.bfloat16
@@ -77,10 +79,10 @@
     result,
     stream, rec_in, gate_in, taps, small_maps, large_maps, channel_decay, extra, n1g, n1b, n2g, n2b,
     ids, wts, in_sem,
-    padded, halo, carry_own, carry_in, wdense, w_in, out_w, w_gu, w_d, s_gu, s_d,
-    part, part_in, rows, hid, y_part, x_in, z_out, z_in, moe,
+    padded, halo, carry_own, carry_in, wdense, w_in, w_rows, out_w, w_gu, w_d, s_gu, s_d,
+    part, pair_in, pair_out, part_in, rows, hid, y_own, y_out, x_in, z_out, z_in, moe,
     local_sem, halo_sem, carry_send, carry_recv, w_send, w_recv,
-    wt_send, wt_recv, tp_send, tp_recv, ag_send, ag_recv, fw_send, fw_recv,
+    wt_send, wt_recv, pair_send, pair_recv, tp_send, tp_recv, right_send, left_send, fw_send, ag_recv,
     xs_send, xs_recv, zs_send, zs_recv,
 ):
     sp_n, tp_n, inner = dims
@@ -95,9 +97,17 @@
     mate = yi * 2 + (1 - half_c)
     length = rec_in.shape[0]
     chans = rec_in.shape[1] * rec_in.shape[2]
-    quarter = stream.shape[0]
+    quarter, width = stream.shape
     fe = rg_hbm.shape[1]
     fs = sg_hbm.shape[1]
+    cut = width // COLUMN_CUTS
+    half_w = width // SPLITS
+
+    def remote(src, dst, send, recv, where):
+        return pltpu.make_async_remote_copy(
+            src_ref=src, dst_ref=dst, send_sem=send, recv_sem=recv,
+            device_id=where, device_id_type=MESH,
+        )
 
     loads = [
         pltpu.make_async_copy(src, dst, in_sem.at[i])
@@ -122,25 +132,73 @@
         pl.semaphore_signal(
             barrier, inc=1, device_id=(sp, lax.rem(tp + step, tp_n)), device_id_type=MESH
         )
+
+    depth = rg_hbm.shape[0] // ROW_CUTS
+    pieces = [(kind, part_id) for part_id in range(ROW_CUTS) for kind in (0, 1)]
+    gate_pieces = len(pieces)
+    pieces += [(2, part_id) for part_id in range(COLUMN_CUTS)]
+
+    def weight_src(piece):
+        kind, part_id = pieces[piece]
+        if kind == 2:
+            return rd_hbm.at[:, pl.ds(part_id * cut, cut)]
+        return (rg_hbm, ru_hbm)[kind].at[pl.ds(part_id * depth, depth)]
+
+    def weight_dst(slot, piece):
+        kind, part_id = pieces[piece]
+        if kind == 2:
+            return w_d.at[part_id, slot]
+        return w_gu.at[slot, pl.ds(part_id * depth, depth), pl.ds(kind * fe, fe)]
+
+    def weight_out(piece, step):
+        return remote(
+            weight_src(piece), weight_dst(tp, piece),
+            wt_send.at[piece, step], wt_recv.at[piece, tp],
+            (sp, lax.rem(yi + step, pairs) * 2 + half_c),
+        )
+
+    def weight_mate(piece, slot, step):
+        src = weight_src(piece) if step == 0 else weight_dst(slot, piece)
+        return remote(
+            src, weight_dst(slot, piece),
+            wt_send.at[piece, pairs + step], wt_recv.at[piece, slot], (sp, mate),
+        )
+
+    def pair_slot(step):
+        return lax.rem(yi + step, pairs) * 2 + half_c
+
+    def weight_arrival(piece, slot):
+        return remote(
+            weight_dst(slot, piece), weight_dst(slot, piece),
+            wt_send.at[piece, 0], wt_recv.at[piece, slot], (sp, mate),
+        )
+
+    def relay(piece):
+        for step in range(1, pairs):
+            weight_arrival(piece, pair_slot(step)).wait_recv()
+            weight_mate(piece, pair_slot(step), step).start()
+
+    def from_mate(piece):
+        for step in range(pairs):
+            weight_arrival(piece, lax.rem(yi + step, pairs) * 2 + 1 - half_c).wait_recv()
+
+    locals_ = [pltpu.make_async_copy(out_w_hbm, out_w, local_sem.at[0])]
+    locals_ += [
+        pltpu.make_async_copy(weight_src(piece), weight_dst(tp, piece), local_sem.at[4 + piece])
+        for piece in range(len(pieces))
+    ]
+    shared_loads = [
+        pltpu.make_async_copy(sg_hbm, s_gu.at[:, pl.ds(0, fs)], local_sem.at[1]),
+        pltpu.make_async_copy(su_hbm, s_gu.at[:, pl.ds(fs, fs)], local_sem.at[2]),
+        pltpu.make_async_copy(sd_hbm, s_d, local_sem.at[3]),
+    ]
+    for load in locals_:
+        load.start()
+    for load in shared_loads:
+        load.start()
     for load in loads:
         load.wait()
     pl.semaphore_wait(barrier, sp_n - 1 + tp_n - 1)
-
-    def remote(src, dst, send, recv, where):
-        return pltpu.make_async_remote_copy(
-            src_ref=src, dst_ref=dst, send_sem=send, recv_sem=recv,
-            device_id=where, device_id_type=MESH,
-        )
-
-    locals_ = [
-        pltpu.make_async_copy(rg_hbm, w_gu.at[tp, :, pl.ds(0, fe)], local_sem.at[0]),
-        pltpu.make_async_copy(ru_hbm, w_gu.at[tp, :, pl.ds(fe, fe)], local_sem.at[1]),
-        pltpu.make_async_copy(rd_hbm, w_d.at[tp], local_sem.at[2]),
-        pltpu.make_async_copy(out_w_hbm, out_w, local_sem.at[3]),
-        pltpu.make_async_copy(sg_hbm, s_gu.at[:, pl.ds(0, fs)], local_sem.at[4]),
-        pltpu.make_async_copy(su_hbm, s_gu.at[:, pl.ds(fs, fs)], local_sem.at[5]),
-        pltpu.make_async_copy(sd_hbm, s_d, local_sem.at[6]),
-    ]
 
     halo_copy = remote(
         rec_in.at[pl.ds(length - 8, 8)], halo, halo_sem.at[0], halo_sem.at[1],
@@ -151,48 +209,11 @@
     def _():
         halo_copy.start()
 
-    depth = rg_hbm.shape[0] // 2
-    fe_half = fe // 2
-
-    def weight_src(piece):
-        kind, part_id = piece // 2, piece % 2
-        if kind == 2:
-            return rd_hbm.at[pl.ds(part_id * fe_half, fe_half)]
-        return (rg_hbm, ru_hbm)[kind].at[pl.ds(part_id * depth, depth)]
-
-    def weight_dst(slot, piece):
-        kind, part_id = piece // 2, piece % 2
-        if kind == 2:
-            return w_d.at[slot, pl.ds(part_id * fe_half, fe_half)]
-        return w_gu.at[slot, pl.ds(part_id * depth, depth), pl.ds(kind * fe, fe)]
-
-    def weight_out(kind, step):
-        return remote(
-            weight_src(kind), weight_dst(tp, kind),
-            wt_send.at[kind, step], wt_recv.at[kind, tp],
-            (sp, lax.rem(yi + step, pairs) * 2 + half_c),
-        )
-
-    def weight_mate(kind, slot, step):
-        src = weight_src(kind) if step == 0 else weight_dst(slot, kind)
-        return remote(
-            src, weight_dst(slot, kind),
-            wt_send.at[kind, pairs + step], wt_recv.at[kind, slot], (sp, mate),
-        )
-
-    def pair_slot(step):
-        return lax.rem(yi + step, pairs) * 2 + half_c
-
     for piece in range(EARLY):
         for step in range(1, pairs):
             weight_out(piece, step).start()
-    locals_[3].start()
-    for piece in range(PIECES):
+    for piece in range(len(pieces)):
         weight_mate(piece, tp, 0).start()
-    for i in range(3):
-        locals_[i].start()
-    for i in (4, 5, 6):
-        locals_[i].start()
 
     expert = lax.broadcasted_iota(jnp.int32, (wdense.shape[0], length), 0)
     table = jnp.zeros((wdense.shape[0], length), F32)
@@ -205,10 +226,6 @@
         return remote(
             wdense, w_in.at[sp], w_send.at[step], w_recv.at[sp], (lax.rem(sp + step, sp_n), tp)
         )
-
-    @pl.loop(1, sp_n)
-    def _(step):
-        w_out(step).start()
 
     small_blocks, large_blocks = lane_blocks(small_maps), lane_blocks(large_maps)
     rate_rows = -8.0 * softplus(-channel_decay[...])
@@ -268,10 +285,16 @@
         )
 
     @pl.loop(1, sp_n)
-    def _(step):
+    def _(back):
+        step = sp_n - back
+
         @pl.when(sp + step < sp_n)
         def _():
             carry_out(step).start()
+
+    @pl.loop(1, sp_n)
+    def _(step):
+        w_out(step).start()
 
     gi = gate_in[...].astype(F32).reshape(length, chans)
     gelu = 0.5 * gi * (1.0 + jnp.tanh(0.7978845608028654 * (gi + 0.044715 * gi * gi * gi)))
@@ -283,70 +306,111 @@
 
     incoming = lax.fori_loop(0, sp, fold, jnp.zeros((1, chans), F32))
     branch = (gelu * (state + decay * incoming)).astype(BF16)
-    locals_[3].wait()
+    locals_[0].wait()
     part[...] = dot(branch, out_w[...]).astype(BF16).reshape(part.shape)
 
+    def pair_copy(step):
+        slot = lax.rem(yi + step, pairs) * 2 + 1 - half_c
+        return remote(
+            part.at[slot], pair_in.at[step], pair_send.at[step], pair_recv.at[step], (sp, mate)
+        )
+
     def part_out(step):
-        to = lax.rem(tp + step, tp_n)
-        return remote(
-            part.at[to], part_in.at[tp], tp_send.at[step], tp_recv.at[tp], (sp, to)
+        to = lax.rem(yi + step, pairs)
+        return remote(
+            pair_out.at[step], part_in.at[yi], tp_send.at[step], tp_recv.at[yi],
+            (sp, to * 2 + half_c),
         )
 
     def part_arrival(who):
-        return remote(part.at[who], part_in.at[who], tp_send.at[0], tp_recv.at[who], (sp, tp))
-
-    for step in range(1, tp_n):
+        return remote(
+            pair_out.at[0], part_in.at[who], tp_send.at[0], tp_recv.at[who], (sp, mate)
+        )
+
+    for step in range(1, pairs + 1):
+        pair_copy(step % pairs).start()
+    for step in range(1, pairs):
+        pair_copy(step).wait_recv()
+        pair_out[step] = (
+            part[pair_slot(step)].astype(F32) + pair_in[step].astype(F32)
+        ).astype(BF16)
         part_out(step).start()
-    for piece in range(EARLY, PIECES):
+    for piece in range(EARLY, len(pieces)):
         for step in range(1, pairs):
             weight_out(piece, step).start()
-    mixed = part[tp].astype(F32)
-    for step in range(1, tp_n):
-        who = lax.rem(tp + step, tp_n)
+    for piece in range(EARLY):
+        relay(piece)
+    pair_copy(0).wait_recv()
+    mixed = part[tp].astype(F32) + pair_in[0].astype(F32)
+    for step in range(1, pairs):
+        who = lax.rem(yi + step, pairs)
         part_arrival(who).wait_recv()
         mixed = mixed + part_in[who].astype(F32)
     normed = layer_norm(
         RESIDUAL_SCALE * stream[...].astype(F32) + mixed, n1g[...], n1b[...]
     ).astype(BF16)
-    rows[sp] = normed
-
-    def ag_out(step):
-        return remote(
-            rows.at[sp], rows.at[sp], ag_send.at[step], ag_recv.at[sp],
-            (lax.rem(zi + step, outer) * inner + xi, tp),
-        )
-
-    def ag_arrival(who):
-        return remote(rows.at[who], rows.at[who], ag_send.at[0], ag_recv.at[who], (sp, tp))
-
-    def forward(who):
-        return remote(
-            rows.at[who], rows.at[who], fw_send.at[who], ag_recv.at[who], (x_peer, tp)
-        )
+    rows[xi, zi] = normed
+
+    def row_piece(col, zj, h):
+        return rows.at[col, zj, :, pl.ds(h * half_w, half_w)]
+
+    def row_copy(zj, h, sems, where):
+        piece = row_piece(xi, zj, h)
+        return remote(piece, piece, sems.at[zj, h], ag_recv.at[zj * inner + xi, h], (where, tp))
+
+    def row_right(zj, h):
+        return row_copy(zj, h, right_send, (zi + 1) * inner + xi)
+
+    def row_left(zj, h):
+        return row_copy(zj, h, left_send, (zi - 1) * inner + xi)
+
+    def row_across(zj, h):
+        return row_copy(zj, h, fw_send, x_peer)
+
+    def row_arrival(col, zj, h):
+        piece = row_piece(col, zj, h)
+        return remote(
+            piece, piece, fw_send.at[zj, h], ag_recv.at[zj * inner + col, h], (x_peer, tp)
+        )
+
+    for h in range(SPLITS):
+        @pl.when(zi + 1 < outer)
+        def _():
+            row_right(zi, h).start()
+
+        @pl.when(zi > 0)
+        def _():
+            row_left(zi, h).start()
+
+        row_across(zi, h).start()
 
     @pl.loop(1, outer)
     def _(step):
-        ag_out(step).start()
-
-    forward(sp).start()
-
-    def weight_arrival(kind, slot):
-        return remote(
-            weight_dst(slot, kind), weight_dst(slot, kind),
-            wt_send.at[kind, 0], wt_recv.at[kind, slot], (sp, mate),
-        )
-
-    def relay(piece):
-        for step in range(1, pairs):
-            weight_arrival(piece, pair_slot(step)).wait_recv()
-            weight_mate(piece, pair_slot(step), step).start()
-
-    for piece in range(EARLY):
+        for h in range(SPLITS):
+            @pl.when(zi - step >= 0)
+            def _():
+                row_arrival(xi, zi - step, h).wait_recv()
+
+                @pl.when(zi + 1 < outer)
+                def _():
+                    row_right(zi - step, h).start()
+
+                row_across(zi - step, h).start()
+
+            @pl.when(zi + step < outer)
+            def _():
+                row_arrival(xi, zi + step, h).wait_recv()
+
+                @pl.when(zi > 0)
+                def _():
+                    row_left(zi + step, h).start()
+
+                row_across(zi + step, h).start()
+
+    for piece in range(EARLY, gate_pieces):
         relay(piece)
-
-    locals_[4].wait()
-    locals_[5].wait()
-    locals_[6].wait()
+    for load in shared_loads:
+        load.wait()
     up = dot(normed, s_gu[...])
     s_hid = (silu(up[:, :fs]) * up[:, fs:]).astype(BF16)
     moe[...] = dot(s_hid, s_d[...]) + RESIDUAL_SCALE * normed.astype(F32)
@@ -356,93 +420,122 @@
         who = lax.rem(sp + step, sp_n)
         remote(wdense, w_in.at[who], w_send.at[0], w_recv.at[who], (sp, tp)).wait_recv()
 
-    for i in range(3):
-        locals_[i].wait()
-
-    @pl.loop(1, outer)
-    def _(step):
-        mine = lax.rem(zi + step, outer) * inner + xi
-        ag_arrival(mine).wait_recv()
-        forward(mine).start()
-
-    for piece in range(EARLY, PIECES):
-        relay(piece)
+    own_rows = lax.broadcasted_iota(jnp.int32, (quarter, length), 0) + tp * quarter
+    pick = lax.broadcasted_iota(jnp.int32, (quarter, length), 1) == own_rows
 
     @pl.loop(0, outer)
-    def _(step):
-        ag_arrival(step * inner + other_x).wait_recv()
-
-    for piece in range(PIECES):
-        for step in range(pairs):
-            weight_arrival(piece, lax.rem(yi + step, pairs) * 2 + 1 - half_c).wait_recv()
-
-    width = stream.shape[1]
-    grp = inner * quarter
-    batch = min(sp_n, 8)
-
-    @pl.loop(0, sp_n // batch)
-    def _(i):
-        block = rows[pl.ds(i * batch, batch)].reshape(batch * quarter, width)
+    def _(zj):
+        for j in range(inner):
+            line = w_in[zj * inner + j, pl.ds(sp, 1)]
+            weight = jnp.sum(jnp.where(pick, line, 0.0), axis=1, keepdims=True)
+            w_rows[j, zj] = jnp.broadcast_to(weight, (quarter, LANES))
+
+    for load in locals_[1 : 1 + gate_pieces]:
+        load.wait()
+    for piece in range(gate_pieces):
+        from_mate(piece)
+
+    batch = min(outer, 4)
+
+    def gate_up(col, i):
+        block = rows[col, pl.ds(i * batch, batch)].reshape(batch * quarter, width)
         for t in range(tp_n):
             gu = dot(block, w_gu[t])
             act = (silu(gu[:, :fe]) * gu[:, fe:]).astype(BF16)
-            hid[pl.ds(i * batch, batch), :, t * fe : (t + 1) * fe] = act.reshape(
+            hid[col, pl.ds(i * batch, batch), :, t * fe : (t + 1) * fe] = act.reshape(
                 batch, quarter, fe
             )
 
-    def x_out(zj):
-        return remote(
-            y_part.at[zj * inner + other_x], x_in.at[zj], xs_send.at[zj], xs_recv.at[zj],
-            (x_peer, tp),
-        )
-
-    own_rows = lax.broadcasted_iota(jnp.int32, (quarter, length), 0) + tp * quarter
-    pick = lax.broadcasted_iota(jnp.int32, (quarter, length), 1) == own_rows
-
-    @pl.loop(1, outer + 1)
-    def _(step):
+    @pl.loop(0, outer // batch)
+    def _(i):
+        gate_up(xi, i)
+
+    @pl.loop(0, outer)
+    def _(zj):
+        for h in range(SPLITS):
+            row_arrival(other_x, zj, h).wait_recv()
+
+    @pl.loop(0, outer // batch)
+    def _(i):
+        gate_up(other_x, i)
+
+    def x_out(c, zj):
+        return remote(
+            y_out.at[c, zj], x_in.at[c, zj], xs_send.at[c, zj], xs_recv.at[c, zj], (x_peer, tp)
+        )
+
+    def z_send(c, step):
         zj = lax.rem(zi + step, outer)
-        block = hid[pl.ds(zj * inner, inner)].reshape(grp, tp_n * fe)
-        value = dot(block, w_d[...].reshape(tp_n * fe, width))
-        for j in range(inner):
-            line = w_in[zj * inner + j, pl.ds(sp, 1)]
-            weight = jnp.sum(jnp.where(pick, line, 0.0), axis=1, keepdims=True)
-            y_part[zj * inner + j] = (
-                weight * value[j * quarter : (j + 1) * quarter]
-            ).astype(BF16)
-        x_out(zj).start()
-
-    def z_send(step):
-        zj = lax.rem(zi + step, outer)
-        return remote(
-            z_out.at[zj], z_in.at[zi], zs_send.at[step], zs_recv.at[zi], (zj * inner + xi, tp)
-        )
-
-    @pl.loop(1, outer)
-    def _(step):
-        zj = lax.rem(zi + step, outer)
-        x_out(zj).wait_recv()
-        both = y_part[zj * inner + xi].astype(F32) + x_in[zj].astype(F32)
-        z_out[zj] = both.astype(BF16)
-        z_send(step).start()
-
-    x_out(zi).wait_recv()
-    moe[...] += y_part[sp].astype(F32) + x_in[zi].astype(F32)
-
-    @pl.loop(1, outer)
-    def _(step):
-        zj = lax.rem(zi + step, outer)
-        remote(z_out.at[zj], z_in.at[zj], zs_send.at[0], zs_recv.at[zj], (sp, tp)).wait_recv()
-        moe[...] += z_in[zj].astype(F32)
+        return remote(
+            z_out.at[c, zj], z_in.at[c, zi], zs_send.at[c, step], zs_recv.at[c, zi],
+            (zj * inner + xi, tp),
+        )
+
+    def down(c, col, dest):
+        @pl.loop(0, outer // batch)
+        def _(i):
+            block = hid[col, pl.ds(i * batch, batch)].reshape(batch * quarter, tp_n * fe)
+            value = dot(block, w_d[c].reshape(tp_n * fe, cut))
+            weight = w_rows[col, pl.ds(i * batch, batch)].reshape(batch * quarter, LANES)
+            for a in range(0, cut, LANES):
+                dest[c, pl.ds(i * batch, batch), :, a : a + LANES] = (
+                    (weight * value[:, a : a + LANES])
+                    .astype(dest.dtype)
+                    .reshape(batch, quarter, LANES)
+                )
+
+    def merge(c):
+        @pl.loop(1, outer)
+        def _(step):
+            zj = lax.rem(zi + step, outer)
+            x_out(c, zj).wait_recv()
+            z_out[c, zj] = (y_own[c, zj].astype(F32) + x_in[c, zj].astype(F32)).astype(BF16)
+            z_send(c, step).start()
+
+    def settle(c):
+        x_out(c, zi).wait_recv()
+        here = moe[:, c * cut : (c + 1) * cut] + (
+            y_own[c, zi].astype(F32) + x_in[c, zi].astype(F32)
+        )
+        moe[:, c * cut : (c + 1) * cut] = here
+
+    for c in range(COLUMN_CUTS):
+        piece = gate_pieces + c
+        relay(piece)
+        locals_[1 + piece].wait()
+        from_mate(piece)
+        down(c, other_x, y_out)
+
+        @pl.loop(1, outer + 1)
+        def _(step):
+            x_out(c, lax.rem(zi + step, outer)).start()
+
+        down(c, xi, y_own)
+        if c:
+            merge(c - 1)
+            settle(c - 1)
+    merge(COLUMN_CUTS - 1)
+    settle(COLUMN_CUTS - 1)
+
+    for c in range(COLUMN_CUTS):
+        @pl.loop(1, outer)
+        def _(step):
+            zj = lax.rem(zi + step, outer)
+            remote(
+                z_out.at[c, zj], z_in.at[c, zj], zs_send.at[c, 0], zs_recv.at[c, zj], (sp, tp)
+            ).wait_recv()
+            moe[:, c * cut : (c + 1) * cut] += z_in[c, zj].astype(F32)
 
     result[...] = layer_norm(moe[...], n2g[...], n2b[...]).astype(BF16)
 
-    for kind in range(PIECES):
+    for piece in range(len(pieces)):
         for step in range(1, pairs):
-            weight_out(kind, step).wait_send()
-            weight_mate(kind, pair_slot(step), step).wait_send()
-        weight_mate(kind, tp, 0).wait_send()
-    for step in range(1, tp_n):
+            weight_out(piece, step).wait_send()
+            weight_mate(piece, pair_slot(step), step).wait_send()
+        weight_mate(piece, tp, 0).wait_send()
+    for step in range(pairs):
+        pair_copy(step).wait_send()
+    for step in range(1, pairs):
         part_out(step).wait_send()
 
     @pl.loop(1, sp_n)
@@ -457,15 +550,25 @@
     def _():
         halo_copy.wait_send()
 
+    @pl.loop(0, outer)
+    def _(zj):
+        for h in range(SPLITS):
+            @pl.when(jnp.logical_and(zj <= zi, zi + 1 < outer))
+            def _():
+                row_right(zj, h).wait_send()
+
+            @pl.when(jnp.logical_and(zj >= zi, zi > 0))
+            def _():
+                row_left(zj, h).wait_send()
+
+            row_across(zj, h).wait_send()
+        for c in range(COLUMN_CUTS):
+            x_out(c, zj).wait_send()
+
     @pl.loop(1, outer)
     def _(step):
-        ag_out(step).wait_send()
-        z_send(step).wait_send()
-
-    @pl.loop(0, outer)
-    def _(step):
-        forward(step * inner + xi).wait_send()
-        x_out(step).wait_send()
+        for c in range(COLUMN_CUTS):
+            z_send(c, step).wait_send()
 
 
 def shards(
@@ -505,6 +608,8 @@
     dma = pltpu.SemaphoreType.DMA
     block = (quarter, width)
     pairs = tp_n // 2
+    cut = width // COLUMN_CUTS
+    pieces = 2 * ROW_CUTS + COLUMN_CUTS
     operands = (
         stream,
         recurrence_input,
@@ -547,38 +652,37 @@
             pltpu.VMEM((sp_n, 2, chans), F32),
             pltpu.VMEM((sp_n, length), F32),
             pltpu.VMEM((sp_n, sp_n, length), F32),
+            pltpu.VMEM((inner, outer, quarter, LANES), F32),
             pltpu.VMEM((chans, width), BF16),
             pltpu.VMEM((tp_n, width, 2 * fe), BF16),
-            pltpu.VMEM((tp_n, fe, width), BF16),
+            pltpu.VMEM((COLUMN_CUTS, tp_n, fe, cut), BF16),
             pltpu.VMEM((width, 2 * fs), BF16),
             pltpu.VMEM((fs, width), BF16),
             pltpu.VMEM((tp_n,) + block, BF16),
-            pltpu.VMEM((tp_n,) + block, BF16),
-            pltpu.VMEM((sp_n,) + block, BF16),
-            pltpu.VMEM((sp_n, quarter, tp_n * fe), BF16),
-            pltpu.VMEM((sp_n,) + block, BF16),
-            pltpu.VMEM((outer,) + block, BF16),
-            pltpu.VMEM((outer,) + block, BF16),
-            pltpu.VMEM((outer,) + block, BF16),
+            pltpu.VMEM((pairs,) + block, BF16),
+            pltpu.VMEM((pairs,) + block, BF16),
+            pltpu.VMEM((pairs,) + block, BF16),
+            pltpu.VMEM((inner, outer) + block, BF16),
+            pltpu.VMEM((inner, outer, quarter, tp_n * fe), BF16),
+            *(pltpu.VMEM((COLUMN_CUTS, outer, quarter, cut), BF16) for _ in range(5)),
             pltpu.VMEM(block, F32),
-            dma((8,)),
+            dma((4 + pieces,)),
             dma((2,)),
             dma((sp_n,)),
             dma((sp_n,)),
             dma((sp_n,)),
             dma((sp_n,)),
-            dma((PIECES, 2 * pairs)),
-            dma((PIECES, tp_n)),
-            dma((tp_n,)),
-            dma((tp_n,)),
-            dma((outer,)),
-            dma((sp_n,)),
-            dma((sp_n,)),
-            dma((1,)),
-            dma((outer,)),
-            dma((outer,)),
-            dma((outer,)),
-            dma((outer,)),
+            dma((pieces, 2 * pairs)),
+            dma((pieces, tp_n)),
+            dma((pairs,)),
+            dma((pairs,)),
+            dma((pairs,)),
+            dma((pairs,)),
+            dma((outer, SPLITS)),
+            dma((outer, SPLITS)),
+            dma((outer, SPLITS)),
+            dma((sp_n, SPLITS)),
+            *(dma((COLUMN_CUTS, outer)) for _ in range(4)),
         ],
         compiler_params=pltpu.CompilerParams(
             has_side_effects=True, collective_id=0, vmem_limit_bytes=limit

time: 72.4 us -> 59.2 us (0.82)
  Pallas kernels: 71.6 us -> 58.4 us
    pallas_call x1, Pallas kernels: 71.6 us -> 58.4 us  [shards(): pl.pallas_call(functools.partial(kernel, dims), out_shape=jax.ShapeDtypeS...]
where the time goes in v2:
time: 59.2 us; the launch traced here: 59.1 us
  Pallas kernels  58.4 us (99%)
  local copies, waits for them, and re-layouts  0.66 us (1%)
    pallas_call x1, Pallas kernels, shards(): pl.pallas_call(functools.partial(kernel, dims), out_shape=jax.ShapeDtypeS...  58.4 us

profile of v2, /device:TPU:0, one launch (start us, length us, event | category | flops | bytes accessed | tf_op | source)
XLA Modules:
  0.0 59.1 jit_solution(18039238538086284745)
XLA Ops:
  0.0 58.4 %shard_map.199 = bf16[32,2048]{1,0:T(8,128)(2,1)S(1)} custom-call(bf16[32,2048]{1,0:T(8,128)(2,1)} %stream_hbm.1, bf16[128,2,256]{2,1,0:T(2,128)(2,1)} %rec_hbm.1, bf16[128,2,256]{2,1,0:T(2,128)(2,1)} %gate_hbm.1, bf16[4,2,256]{2,1,0:T(2,128)(2,1)} %taps_hbm.1, bf16[2,4,64,64]{3,2,1,0:T(8,128)(2,1)} %small_hbm.1, bf16[2,2,128,128]{3,2,1,0:T(8,128)(2,1)} %large_hbm.1, ...), custom_call_target="tpu_custom_call" | custom-call | tf_op jit(solution)/shard_map/pallas_call | solution.py:641
  58.4 0.7 %copy.23 = bf16[32,2048]{1,0:T(8,128)(2,1)} copy(bf16[32,2048]{1,0:T(8,128)(2,1)S(1)} %shard_map.199) | data formatting | bytes 262144

commit v3 on v2

--- a/solution.py
+++ b/solution.py
@@ -11,8 +11,8 @@
 NORM_EPSILON = 1e-05
 LANES = 128
 ROW_CUTS = 4
-COLUMN_CUTS = 4
-EARLY = 4
+COLUMN_CUTS = (2, 2, 2, 2, 2, 2, 2, 2)
+EARLY = (3, 1)
 SPLITS = 2
 MESH = pl.DeviceIdType.MESH
 F32 = jnp.float32
@@ -80,9 +80,10 @@
     stream, rec_in, gate_in, taps, small_maps, large_maps, channel_decay, extra, n1g, n1b, n2g, n2b,
     ids, wts, in_sem,
     padded, halo, carry_own, carry_in, wdense, w_in, w_rows, out_w, w_gu, w_d, s_gu, s_d,
-    part, pair_in, pair_out, part_in, rows, hid, y_own, y_out, x_in, z_out, z_in, moe,
+    part, pair_in, pair_out, part_in, rows, hid, gu_acc, y_own, y_out, x_in, z_out, z_in, moe,
     local_sem, halo_sem, carry_send, carry_recv, w_send, w_recv,
-    wt_send, wt_recv, pair_send, pair_recv, tp_send, tp_recv, right_send, left_send, fw_send, ag_recv,
+    out_send, own_send, relay_send, own_recv, far_recv, relay_recv, pair_send, pair_recv,
+    tp_send, tp_recv, right_send, left_send, fw_send, ag_recv, agx_recv,
     xs_send, xs_recv, zs_send, zs_recv,
 ):
     sp_n, tp_n, inner = dims
@@ -100,13 +101,28 @@
     quarter, width = stream.shape
     fe = rg_hbm.shape[1]
     fs = sg_hbm.shape[1]
-    cut = width // COLUMN_CUTS
+    unit = width // sum(COLUMN_CUTS)
+    spans = []
+    for c in range(len(COLUMN_CUTS)):
+        spans.append((sum(COLUMN_CUTS[:c]) * unit, COLUMN_CUTS[c] * unit))
     half_w = width // SPLITS
 
     def remote(src, dst, send, recv, where):
         return pltpu.make_async_remote_copy(
             src_ref=src, dst_ref=dst, send_sem=send, recv_sem=recv,
             device_id=where, device_id_type=MESH,
+        )
+
+    barrier = pltpu.get_barrier_semaphore()
+    for step in range(1, tp_n):
+        pl.semaphore_signal(
+            barrier, inc=1, device_id=(sp, lax.rem(tp + step, tp_n)), device_id_type=MESH
+        )
+
+    @pl.loop(1, sp_n)
+    def _(step):
+        pl.semaphore_signal(
+            barrier, inc=1, device_id=(lax.rem(sp + step, sp_n), tp), device_id_type=MESH
         )
 
     loads = [
@@ -120,100 +136,106 @@
     ]
     for load in loads:
         load.start()
-    barrier = pltpu.get_barrier_semaphore()
-
-    @pl.loop(1, sp_n)
-    def _(step):
-        pl.semaphore_signal(
-            barrier, inc=1, device_id=(lax.rem(sp + step, sp_n), tp), device_id_type=MESH
-        )
-
-    for step in range(1, tp_n):
-        pl.semaphore_signal(
-            barrier, inc=1, device_id=(sp, lax.rem(tp + step, tp_n)), device_id_type=MESH
-        )
 
     depth = rg_hbm.shape[0] // ROW_CUTS
     pieces = [(kind, part_id) for part_id in range(ROW_CUTS) for kind in (0, 1)]
     gate_pieces = len(pieces)
-    pieces += [(2, part_id) for part_id in range(COLUMN_CUTS)]
+    pieces += [(2, part_id) for part_id in range(len(spans))]
 
     def weight_src(piece):
         kind, part_id = pieces[piece]
         if kind == 2:
-            return rd_hbm.at[:, pl.ds(part_id * cut, cut)]
+            return rd_hbm.at[:, pl.ds(*spans[part_id])]
         return (rg_hbm, ru_hbm)[kind].at[pl.ds(part_id * depth, depth)]
 
     def weight_dst(slot, piece):
         kind, part_id = pieces[piece]
         if kind == 2:
-            return w_d.at[part_id, slot]
+            return w_d.at[slot, :, pl.ds(*spans[part_id])]
         return w_gu.at[slot, pl.ds(part_id * depth, depth), pl.ds(kind * fe, fe)]
 
+    def stage_ref(slot, stage):
+        if stage < ROW_CUTS:
+            return w_gu.at[slot, pl.ds(stage * depth, depth)]
+        return w_d.at[slot, :, pl.ds(*spans[stage - ROW_CUTS])]
+
+    def weight_all(slot, down):
+        return (w_d if down else w_gu).at[slot]
+
     def weight_out(piece, step):
+        kind, part_id = pieces[piece]
+        stage = ROW_CUTS + part_id if kind == 2 else part_id
         return remote(
             weight_src(piece), weight_dst(tp, piece),
-            wt_send.at[piece, step], wt_recv.at[piece, tp],
+            out_send.at[kind // 2, step - 1], far_recv.at[stage, step - 1],
             (sp, lax.rem(yi + step, pairs) * 2 + half_c),
-        )
-
-    def weight_mate(piece, slot, step):
-        src = weight_src(piece) if step == 0 else weight_dst(slot, piece)
-        return remote(
-            src, weight_dst(slot, piece),
-            wt_send.at[piece, pairs + step], wt_recv.at[piece, slot], (sp, mate),
         )
 
     def pair_slot(step):
         return lax.rem(yi + step, pairs) * 2 + half_c
 
-    def weight_arrival(piece, slot):
-        return remote(
-            weight_dst(slot, piece), weight_dst(slot, piece),
-            wt_send.at[piece, 0], wt_recv.at[piece, slot], (sp, mate),
-        )
-
-    def relay(piece):
+    def far_arrival(stage, step):
+        block = stage_ref(pair_slot(step), stage)
+        return remote(
+            block, block, out_send.at[0, 0], far_recv.at[stage, pairs - step - 1], (sp, mate)
+        )
+
+    def stage_mate(stage, step):
+        block = stage_ref(pair_slot(step), stage)
+        return remote(
+            block, block, relay_send.at[int(stage >= ROW_CUTS), step - 1],
+            relay_recv.at[stage, step - 1], (sp, mate),
+        )
+
+    def relay_arrival(stage, step):
+        block = stage_ref(lax.rem(yi + step, pairs) * 2 + 1 - half_c, stage)
+        return remote(
+            block, block, relay_send.at[0, 0], relay_recv.at[stage, step - 1], (sp, mate)
+        )
+
+    def relay(stage):
         for step in range(1, pairs):
-            weight_arrival(piece, pair_slot(step)).wait_recv()
-            weight_mate(piece, pair_slot(step), step).start()
-
-    def from_mate(piece):
-        for step in range(pairs):
-            weight_arrival(piece, lax.rem(yi + step, pairs) * 2 + 1 - half_c).wait_recv()
-
-    locals_ = [pltpu.make_async_copy(out_w_hbm, out_w, local_sem.at[0])]
-    locals_ += [
-        pltpu.make_async_copy(weight_src(piece), weight_dst(tp, piece), local_sem.at[4 + piece])
-        for piece in range(len(pieces))
+            far_arrival(stage, step).wait_recv()
+            stage_mate(stage, step).start()
+
+    def from_mate(stage):
+        for step in range(1, pairs):
+            relay_arrival(stage, step).wait_recv()
+
+    own_weights = [
+        (rg_hbm, w_gu.at[tp, :, pl.ds(0, fe)], 0),
+        (ru_hbm, w_gu.at[tp, :, pl.ds(fe, fe)], 0),
+        (rd_hbm, w_d.at[tp], 1),
     ]
-    shared_loads = [
-        pltpu.make_async_copy(sg_hbm, s_gu.at[:, pl.ds(0, fs)], local_sem.at[1]),
-        pltpu.make_async_copy(su_hbm, s_gu.at[:, pl.ds(fs, fs)], local_sem.at[2]),
-        pltpu.make_async_copy(sd_hbm, s_d, local_sem.at[3]),
-    ]
-    for load in locals_:
-        load.start()
-    for load in shared_loads:
-        load.start()
-    for load in loads:
-        load.wait()
-    pl.semaphore_wait(barrier, sp_n - 1 + tp_n - 1)
-
     halo_copy = remote(
         rec_in.at[pl.ds(length - 8, 8)], halo, halo_sem.at[0], halo_sem.at[1],
         (lax.rem(sp + 1, sp_n), tp),
     )
+    pl.semaphore_wait(barrier, sp_n - 1 + tp_n - 1)
+    early = [*range(EARLY[0]), *range(gate_pieces, gate_pieces + EARLY[1])]
+    for piece in early:
+        for step in range(1, pairs):
+            weight_out(piece, step).start()
+    loads[0].wait()
 
     @pl.when(sp + 1 < sp_n)
     def _():
         halo_copy.start()
 
-    for piece in range(EARLY):
-        for step in range(1, pairs):
-            weight_out(piece, step).start()
-    for piece in range(len(pieces)):
-        weight_mate(piece, tp, 0).start()
+    out_w_load = pltpu.make_async_copy(out_w_hbm, out_w, local_sem.at[0])
+    out_w_load.start()
+    for src, dst, down in own_weights:
+        remote(src, dst, own_send.at[down], own_recv.at[down], (sp, mate)).start()
+        pltpu.make_async_copy(src, dst, local_sem.at[1 + down]).start()
+    shared_loads = [
+        pltpu.make_async_copy(sg_hbm, s_gu.at[:, pl.ds(0, fs)], local_sem.at[3]),
+        pltpu.make_async_copy(su_hbm, s_gu.at[:, pl.ds(fs, fs)], local_sem.at[4]),
+        pltpu.make_async_copy(sd_hbm, s_d, local_sem.at[5]),
+    ]
+    for load in shared_loads:
+        load.start()
+    for load in loads[1:]:
+        load.wait()
 
     expert = lax.broadcasted_iota(jnp.int32, (wdense.shape[0], length), 0)
     table = jnp.zeros((wdense.shape[0], length), F32)
@@ -224,7 +246,7 @@
 
     def w_out(step):
         return remote(
-            wdense, w_in.at[sp], w_send.at[step], w_recv.at[sp], (lax.rem(sp + step, sp_n), tp)
+            wdense, w_in.at[sp], w_send.at[0], w_recv.at[0], (lax.rem(sp + step, sp_n), tp)
         )
 
     small_blocks, large_blocks = lane_blocks(small_maps), lane_blocks(large_maps)
@@ -306,25 +328,26 @@
 
     incoming = lax.fori_loop(0, sp, fold, jnp.zeros((1, chans), F32))
     branch = (gelu * (state + decay * incoming)).astype(BF16)
-    locals_[0].wait()
+    out_w_load.wait()
     part[...] = dot(branch, out_w[...]).astype(BF16).reshape(part.shape)
 
     def pair_copy(step):
         slot = lax.rem(yi + step, pairs) * 2 + 1 - half_c
         return remote(
-            part.at[slot], pair_in.at[step], pair_send.at[step], pair_recv.at[step], (sp, mate)
+            part.at[slot], pair_in.at[step], pair_send.at[0], pair_recv.at[step], (sp, mate)
         )
 
     def part_out(step):
         to = lax.rem(yi + step, pairs)
         return remote(
-            pair_out.at[step], part_in.at[yi], tp_send.at[step], tp_recv.at[yi],
+            pair_out.at[step], part_in.at[yi], tp_send.at[step - 1], tp_recv.at[step - 1],
             (sp, to * 2 + half_c),
         )
 
-    def part_arrival(who):
-        return remote(
-            pair_out.at[0], part_in.at[who], tp_send.at[0], tp_recv.at[who], (sp, mate)
+    def part_arrival(step):
+        who = lax.rem(yi + step, pairs)
+        return remote(
+            pair_out.at[0], part_in.at[who], tp_send.at[0], tp_recv.at[pairs - step - 1], (sp, mate)
         )
 
     for step in range(1, pairs + 1):
@@ -335,16 +358,15 @@
             part[pair_slot(step)].astype(F32) + pair_in[step].astype(F32)
         ).astype(BF16)
         part_out(step).start()
-    for piece in range(EARLY, len(pieces)):
-        for step in range(1, pairs):
-            weight_out(piece, step).start()
-    for piece in range(EARLY):
-        relay(piece)
+    for piece in range(len(pieces)):
+        if piece not in early:
+            for step in range(1, pairs):
+                weight_out(piece, step).start()
     pair_copy(0).wait_recv()
     mixed = part[tp].astype(F32) + pair_in[0].astype(F32)
     for step in range(1, pairs):
         who = lax.rem(yi + step, pairs)
-        part_arrival(who).wait_recv()
+        part_arrival(step).wait_recv()
         mixed = mixed + part_in[who].astype(F32)
     normed = layer_norm(
         RESIDUAL_SCALE * stream[...].astype(F32) + mixed, n1g[...], n1b[...]
@@ -356,22 +378,21 @@
 
     def row_copy(zj, h, sems, where):
         piece = row_piece(xi, zj, h)
-        return remote(piece, piece, sems.at[zj, h], ag_recv.at[zj * inner + xi, h], (where, tp))
+        return remote(piece, piece, sems, ag_recv.at[zj, h], (where, tp))
 
     def row_right(zj, h):
-        return row_copy(zj, h, right_send, (zi + 1) * inner + xi)
+        return row_copy(zj, h, right_send.at[zj], (zi + 1) * inner + xi)
 
     def row_left(zj, h):
-        return row_copy(zj, h, left_send, (zi - 1) * inner + xi)
+        return row_copy(zj, h, left_send.at[zj], (zi - 1) * inner + xi)
 
     def row_across(zj, h):
-        return row_copy(zj, h, fw_send, x_peer)
-
-    def row_arrival(col, zj, h):
-        piece = row_piece(col, zj, h)
-        return remote(
-            piece, piece, fw_send.at[zj, h], ag_recv.at[zj * inner + col, h], (x_peer, tp)
-        )
+        piece = row_piece(xi, zj, h)
+        return remote(piece, piece, fw_send.at[0], agx_recv.at[0], (x_peer, tp))
+
+    def row_arrival(zj, h):
+        piece = row_piece(xi, zj, h)
+        return remote(piece, piece, fw_send.at[0], ag_recv.at[zj, h], (x_peer, tp))
 
     for h in range(SPLITS):
         @pl.when(zi + 1 < outer)
@@ -389,7 +410,7 @@
         for h in range(SPLITS):
             @pl.when(zi - step >= 0)
             def _():
-                row_arrival(xi, zi - step, h).wait_recv()
+                row_arrival(zi - step, h).wait_recv()
 
                 @pl.when(zi + 1 < outer)
                 def _():
@@ -399,7 +420,7 @@
 
             @pl.when(zi + step < outer)
             def _():
-                row_arrival(xi, zi + step, h).wait_recv()
+                row_arrival(zi + step, h).wait_recv()
 
                 @pl.when(zi > 0)
                 def _():
@@ -407,18 +428,16 @@
 
                 row_across(zi + step, h).start()
 
-    for piece in range(EARLY, gate_pieces):
-        relay(piece)
+    for stage in (*range(ROW_CUTS - 1), *range(ROW_CUTS, ROW_CUTS + EARLY[1])):
+        relay(stage)
     for load in shared_loads:
         load.wait()
     up = dot(normed, s_gu[...])
     s_hid = (silu(up[:, :fs]) * up[:, fs:]).astype(BF16)
     moe[...] = dot(s_hid, s_d[...]) + RESIDUAL_SCALE * normed.astype(F32)
 
-    @pl.loop(1, sp_n)
-    def _(step):
-        who = lax.rem(sp + step, sp_n)
-        remote(wdense, w_in.at[who], w_send.at[0], w_recv.at[who], (sp, tp)).wait_recv()
+    tables = w_in.at[pl.ds(0, sp_n - 1)]
+    remote(tables, tables, w_send.at[0], w_recv.at[0], (x_peer, tp)).wait_recv()
 
     own_rows = lax.broadcasted_iota(jnp.int32, (quarter, length), 0) + tp * quarter
     pick = lax.broadcasted_iota(jnp.int32, (quarter, length), 1) == own_rows
@@ -430,118 +449,134 @@
             weight = jnp.sum(jnp.where(pick, line, 0.0), axis=1, keepdims=True)
             w_rows[j, zj] = jnp.broadcast_to(weight, (quarter, LANES))
 
-    for load in locals_[1 : 1 + gate_pieces]:
-        load.wait()
-    for piece in range(gate_pieces):
-        from_mate(piece)
+    for down in (0, 1):
+        own = weight_all(tp, down)
+        pltpu.make_async_copy(own, own, local_sem.at[1 + down]).wait()
+        theirs = weight_all(mate, down)
+        remote(theirs, theirs, own_send.at[down], own_recv.at[down], (sp, mate)).wait_recv()
 
     batch = min(outer, 4)
-
-    def gate_up(col, i):
-        block = rows[col, pl.ds(i * batch, batch)].reshape(batch * quarter, width)
-        for t in range(tp_n):
-            gu = dot(block, w_gu[t])
-            act = (silu(gu[:, :fe]) * gu[:, fe:]).astype(BF16)
-            hid[col, pl.ds(i * batch, batch), :, t * fe : (t + 1) * fe] = act.reshape(
-                batch, quarter, fe
-            )
-
-    @pl.loop(0, outer // batch)
-    def _(i):
-        gate_up(xi, i)
-
-    @pl.loop(0, outer)
-    def _(zj):
-        for h in range(SPLITS):
-            row_arrival(other_x, zj, h).wait_recv()
-
-    @pl.loop(0, outer // batch)
-    def _(i):
-        gate_up(other_x, i)
-
-    def x_out(c, zj):
-        return remote(
-            y_out.at[c, zj], x_in.at[c, zj], xs_send.at[c, zj], xs_recv.at[c, zj], (x_peer, tp)
+    tall = batch * quarter
+
+    def gate_up(col, stage):
+        last = stage == ROW_CUTS - 1
+
+        @pl.loop(0, outer // batch)
+        def _(i):
+            block = rows[
+                col, pl.ds(i * batch, batch), :, stage * depth : (stage + 1) * depth
+            ].reshape(tall, depth)
+            for t in range(tp_n):
+                gu = dot(block, w_gu[t, stage * depth : (stage + 1) * depth])
+                if stage:
+                    gu = gu + gu_acc[col, i, :, t * 2 * fe : (t + 1) * 2 * fe]
+                if last:
+                    act = (silu(gu[:, :fe]) * gu[:, fe:]).astype(BF16)
+                    hid[col, i, :, t * fe : (t + 1) * fe] = act
+                else:
+                    gu_acc[col, i, :, t * 2 * fe : (t + 1) * 2 * fe] = gu
+
+    for stage in range(ROW_CUTS - 1):
+        from_mate(stage)
+        gate_up(xi, stage)
+    side = rows.at[other_x]
+    remote(side, side, fw_send.at[0], agx_recv.at[0], (x_peer, tp)).wait_recv()
+    for stage in range(ROW_CUTS - 1):
+        gate_up(other_x, stage)
+    relay(ROW_CUTS - 1)
+    from_mate(ROW_CUTS - 1)
+    gate_up(other_x, ROW_CUTS - 1)
+    gate_up(xi, ROW_CUTS - 1)
+
+    def columns(ref, c):
+        return ref.at[:, :, pl.ds(*spans[c])]
+
+    def x_out(c):
+        return remote(
+            columns(y_out, c), columns(x_in, c), xs_send.at[0], xs_recv.at[c], (x_peer, tp)
         )
 
     def z_send(c, step):
         zj = lax.rem(zi + step, outer)
         return remote(
-            z_out.at[c, zj], z_in.at[c, zi], zs_send.at[c, step], zs_recv.at[c, zi],
+            columns(z_out, c).at[zj], columns(z_in, c).at[zi], zs_send.at[0], zs_recv.at[c],
             (zj * inner + xi, tp),
         )
 
     def down(c, col, dest):
+        first, wide = spans[c]
+
         @pl.loop(0, outer // batch)
         def _(i):
-            block = hid[col, pl.ds(i * batch, batch)].reshape(batch * quarter, tp_n * fe)
-            value = dot(block, w_d[c].reshape(tp_n * fe, cut))
-            weight = w_rows[col, pl.ds(i * batch, batch)].reshape(batch * quarter, LANES)
-            for a in range(0, cut, LANES):
-                dest[c, pl.ds(i * batch, batch), :, a : a + LANES] = (
+            value = dot(
+                hid[col, i], w_d[:, :, first : first + wide].reshape(tp_n * fe, wide)
+            )
+            weight = w_rows[col, pl.ds(i * batch, batch)].reshape(tall, LANES)
+            for a in range(0, wide, LANES):
+                dest[pl.ds(i * batch, batch), :, first + a : first + a + LANES] = (
                     (weight * value[:, a : a + LANES])
                     .astype(dest.dtype)
                     .reshape(batch, quarter, LANES)
                 )
 
     def merge(c):
+        first, wide = spans[c]
+        at = slice(first, first + wide)
+        x_out(c).wait_recv()
+
         @pl.loop(1, outer)
         def _(step):
             zj = lax.rem(zi + step, outer)
-            x_out(c, zj).wait_recv()
-            z_out[c, zj] = (y_own[c, zj].astype(F32) + x_in[c, zj].astype(F32)).astype(BF16)
+            z_out[zj, :, at] = (
+                y_own[zj, :, at].astype(F32) + x_in[zj, :, at].astype(F32)
+            ).astype(BF16)
             z_send(c, step).start()
 
-    def settle(c):
-        x_out(c, zi).wait_recv()
-        here = moe[:, c * cut : (c + 1) * cut] + (
-            y_own[c, zi].astype(F32) + x_in[c, zi].astype(F32)
-        )
-        moe[:, c * cut : (c + 1) * cut] = here
-
-    for c in range(COLUMN_CUTS):
-        piece = gate_pieces + c
-        relay(piece)
-        locals_[1 + piece].wait()
-        from_mate(piece)
+        moe[:, at] = moe[:, at] + (y_own[zi, :, at].astype(F32) + x_in[zi, :, at].astype(F32))
+
+    chunks = len(spans)
+    ahead = max(EARLY[1], 1)
+    if EARLY[1] == 0:
+        relay(ROW_CUTS)
+    for c in range(chunks):
+        if ahead <= c + 1 < chunks:
+            relay(ROW_CUTS + c + 1)
+        from_mate(ROW_CUTS + c)
         down(c, other_x, y_out)
-
-        @pl.loop(1, outer + 1)
-        def _(step):
-            x_out(c, lax.rem(zi + step, outer)).start()
-
+        x_out(c).start()
         down(c, xi, y_own)
-        if c:
-            merge(c - 1)
-            settle(c - 1)
-    merge(COLUMN_CUTS - 1)
-    settle(COLUMN_CUTS - 1)
-
-    for c in range(COLUMN_CUTS):
+        if c >= 2:
+            merge(c - 2)
+    merge(chunks - 2)
+    merge(chunks - 1)
+
+    for c in range(chunks):
+        first, wide = spans[c]
+        at = slice(first, first + wide)
+        group = columns(z_in, c).at[pl.ds(0, outer - 1)]
+        remote(group, group, zs_send.at[0], zs_recv.at[c], (x_peer, tp)).wait_recv()
+
         @pl.loop(1, outer)
         def _(step):
-            zj = lax.rem(zi + step, outer)
+            moe[:, at] += z_in[lax.rem(zi + step, outer), :, at].astype(F32)
+
+    result[...] = layer_norm(moe[...], n2g[...], n2b[...]).astype(BF16)
+
+    for down in (0, 1):
+        whole = weight_all(tp, down)
+        for step in range(1, pairs):
+            remote(whole, whole, out_send.at[down, step - 1], own_recv.at[0], (sp, mate)).wait_send()
             remote(
-                z_out.at[c, zj], z_in.at[c, zj], zs_send.at[c, 0], zs_recv.at[c, zj], (sp, tp)
-            ).wait_recv()
-            moe[:, c * cut : (c + 1) * cut] += z_in[c, zj].astype(F32)
-
-    result[...] = layer_norm(moe[...], n2g[...], n2b[...]).astype(BF16)
-
-    for piece in range(len(pieces)):
-        for step in range(1, pairs):
-            weight_out(piece, step).wait_send()
-            weight_mate(piece, pair_slot(step), step).wait_send()
-        weight_mate(piece, tp, 0).wait_send()
-    for step in range(pairs):
-        pair_copy(step).wait_send()
+                whole, whole, relay_send.at[down, step - 1], own_recv.at[0], (sp, mate)
+            ).wait_send()
+        remote(whole, whole, own_send.at[down], own_recv.at[0], (sp, mate)).wait_send()
+    remote(pair_in, pair_in, pair_send.at[0], pair_recv.at[0], (sp, mate)).wait_send()
     for step in range(1, pairs):
         part_out(step).wait_send()
+    remote(tables, tables, w_send.at[0], w_recv.at[0], (x_peer, tp)).wait_send()
 
     @pl.loop(1, sp_n)
     def _(step):
-        w_out(step).wait_send()
-
         @pl.when(sp + step < sp_n)
         def _():
             carry_out(step).wait_send()
@@ -552,23 +587,20 @@
 
     @pl.loop(0, outer)
     def _(zj):
-        for h in range(SPLITS):
-            @pl.when(jnp.logical_and(zj <= zi, zi + 1 < outer))
-            def _():
-                row_right(zj, h).wait_send()
-
-            @pl.when(jnp.logical_and(zj >= zi, zi > 0))
-            def _():
-                row_left(zj, h).wait_send()
-
-            row_across(zj, h).wait_send()
-        for c in range(COLUMN_CUTS):
-            x_out(c, zj).wait_send()
-
-    @pl.loop(1, outer)
-    def _(step):
-        for c in range(COLUMN_CUTS):
-            z_send(c, step).wait_send()
+        block = rows.at[xi, zj]
+
+        @pl.when(jnp.logical_and(zj <= zi, zi + 1 < outer))
+        def _():
+            remote(block, block, right_send.at[zj], fw_send.at[0], (x_peer, tp)).wait_send()
+
+        @pl.when(jnp.logical_and(zj >= zi, zi > 0))
+        def _():
+            remote(block, block, left_send.at[zj], fw_send.at[0], (x_peer, tp)).wait_send()
+
+    remote(side, side, fw_send.at[0], agx_recv.at[0], (x_peer, tp)).wait_send()
+    remote(y_out, y_out, xs_send.at[0], agx_recv.at[0], (x_peer, tp)).wait_send()
+    sent = z_out.at[pl.ds(0, outer - 1)]
+    remote(sent, sent, zs_send.at[0], agx_recv.at[0], (x_peer, tp)).wait_send()
 
 
 def shards(
@@ -608,8 +640,8 @@
     dma = pltpu.SemaphoreType.DMA
     block = (quarter, width)
     pairs = tp_n // 2
-    cut = width // COLUMN_CUTS
-    pieces = 2 * ROW_CUTS + COLUMN_CUTS
+    stages = ROW_CUTS + len(COLUMN_CUTS)
+    batch = min(outer, 4)
     operands = (
         stream,
         recurrence_input,
@@ -655,7 +687,7 @@
             pltpu.VMEM((inner, outer, quarter, LANES), F32),
             pltpu.VMEM((chans, width), BF16),
             pltpu.VMEM((tp_n, width, 2 * fe), BF16),
-            pltpu.VMEM((COLUMN_CUTS, tp_n, fe, cut), BF16),
+            pltpu.VMEM((tp_n, fe, width), BF16),
             pltpu.VMEM((width, 2 * fs), BF16),
             pltpu.VMEM((fs, width), BF16),
             pltpu.VMEM((tp_n,) + block, BF16),
@@ -663,26 +695,35 @@
             pltpu.VMEM((pairs,) + block, BF16),
             pltpu.VMEM((pairs,) + block, BF16),
             pltpu.VMEM((inner, outer) + block, BF16),
-            pltpu.VMEM((inner, outer, quarter, tp_n * fe), BF16),
-            *(pltpu.VMEM((COLUMN_CUTS, outer, quarter, cut), BF16) for _ in range(5)),
+            pltpu.VMEM((inner, outer // batch, batch * quarter, tp_n * fe), BF16),
+            pltpu.VMEM((inner, outer // batch, batch * quarter, tp_n * 2 * fe), F32),
+            *(pltpu.VMEM((outer,) + block, BF16) for _ in range(5)),
             pltpu.VMEM(block, F32),
-            dma((4 + pieces,)),
+            dma((6,)),
             dma((2,)),
             dma((sp_n,)),
             dma((sp_n,)),
-            dma((sp_n,)),
-            dma((sp_n,)),
-            dma((pieces, 2 * pairs)),
-            dma((pieces, tp_n)),
+            dma((1,)),
+            dma((1,)),
+            dma((2, pairs - 1)),
+            dma((2,)),
+            dma((2, pairs - 1)),
+            dma((2,)),
+            dma((stages, pairs - 1)),
+            dma((stages, pairs - 1)),
+            dma((1,)),
             dma((pairs,)),
-            dma((pairs,)),
-            dma((pairs,)),
-            dma((pairs,)),
+            dma((pairs - 1,)),
+            dma((pairs - 1,)),
+            dma((outer,)),
+            dma((outer,)),
+            dma((1,)),
             dma((outer, SPLITS)),
-            dma((outer, SPLITS)),
-            dma((outer, SPLITS)),
-            dma((sp_n, SPLITS)),
-            *(dma((COLUMN_CUTS, outer)) for _ in range(4)),
+            dma((1,)),
+            dma((1,)),
+            dma((len(COLUMN_CUTS),)),
+            dma((1,)),
+            dma((len(COLUMN_CUTS),)),
         ],
         compiler_params=pltpu.CompilerParams(
             has_side_effects=True, collective_id=0, vmem_limit_bytes=limit

time: 59.2 us -> 56.9 us (0.961)
  Pallas kernels: 58.4 us -> 56.1 us
    pallas_call x1, Pallas kernels: 58.4 us -> 56.1 us  [shards(): pl.pallas_call(functools.partial(kernel, dims), out_shape=jax.ShapeDtypeS...]
where the time goes in v3:
time: 56.9 us; the launch traced here: 56.8 us
  Pallas kernels  56.1 us (99%)
  local copies, waits for them, and re-layouts  0.66 us (1%)
    pallas_call x1, Pallas kernels, shards(): pl.pallas_call(functools.partial(kernel, dims), out_shape=jax.ShapeDtypeS...  56.1 us

profile of v3, /device:TPU:0, one launch (start us, length us, event | category | flops | bytes accessed | tf_op | source)
XLA Modules:
  0.0 56.8 jit_solution(15773114377269588148)
XLA Ops:
  0.0 56.1 %shard_map.199 = bf16[32,2048]{1,0:T(8,128)(2,1)S(1)} custom-call(bf16[32,2048]{1,0:T(8,128)(2,1)} %stream_hbm.1, bf16[128,2,256]{2,1,0:T(2,128)(2,1)} %rec_hbm.1, bf16[128,2,256]{2,1,0:T(2,128)(2,1)} %gate_hbm.1, bf16[4,2,256]{2,1,0:T(2,128)(2,1)} %taps_hbm.1, bf16[2,4,64,64]{3,2,1,0:T(8,128)(2,1)} %small_hbm.1, bf16[2,2,128,128]{3,2,1,0:T(8,128)(2,1)} %large_hbm.1, ...), custom_call_target="tpu_custom_call" | custom-call | tf_op jit(solution)/shard_map/pallas_call | solution.py:673
  56.1 0.7 %copy.23 = bf16[32,2048]{1,0:T(8,128)(2,1)} copy(bf16[32,2048]{1,0:T(8,128)(2,1)S(1)} %shard_map.199) | data formatting | bytes 262144

commit v4 on v3

--- a/solution.py
+++ b/solution.py
@@ -12,7 +12,7 @@
 LANES = 128
 ROW_CUTS = 4
 COLUMN_CUTS = (2, 2, 2, 2, 2, 2, 2, 2)
-EARLY = (3, 1)
+EARLY = (0, 1, 1, 1)
 SPLITS = 2
 MESH = pl.DeviceIdType.MESH
 F32 = jnp.float32
@@ -79,8 +79,8 @@
     result,
     stream, rec_in, gate_in, taps, small_maps, large_maps, channel_decay, extra, n1g, n1b, n2g, n2b,
     ids, wts, in_sem,
-    padded, halo, carry_own, carry_in, wdense, w_in, w_rows, out_w, w_gu, w_d, s_gu, s_d,
-    part, pair_in, pair_out, part_in, rows, hid, gu_acc, y_own, y_out, x_in, z_out, z_in, moe,
+    padded, halo, carry_own, carry_in, wdense, w_in, w_rows, w_peer, place_out, place_in, out_w, w_gu, w_d, s_gu, s_d,
+    part, pair_in, pair_out, part_in, rows, hid, hid_pack, gu_acc, y_own, y_out, x_in, z_out, z_in, moe,
     local_sem, halo_sem, carry_send, carry_recv, w_send, w_recv,
     out_send, own_send, relay_send, own_recv, far_recv, relay_recv, pair_send, pair_recv,
     tp_send, tp_recv, right_send, left_send, fw_send, ag_recv, agx_recv,
@@ -212,10 +212,14 @@
         (lax.rem(sp + 1, sp_n), tp),
     )
     pl.semaphore_wait(barrier, sp_n - 1 + tp_n - 1)
-    early = [*range(EARLY[0]), *range(gate_pieces, gate_pieces + EARLY[1])]
-    for piece in early:
+    order = [0, 1, gate_pieces, *range(2, gate_pieces), *range(gate_pieces + 1, len(pieces))]
+
+    def send_weights(piece):
         for step in range(1, pairs):
             weight_out(piece, step).start()
+
+    for place, least in enumerate(EARLY):
+        pl.when(zi >= least)(functools.partial(send_weights, order[place]))
     loads[0].wait()
 
     @pl.when(sp + 1 < sp_n)
@@ -358,10 +362,11 @@
             part[pair_slot(step)].astype(F32) + pair_in[step].astype(F32)
         ).astype(BF16)
         part_out(step).start()
-    for piece in range(len(pieces)):
-        if piece not in early:
-            for step in range(1, pairs):
-                weight_out(piece, step).start()
+    for place, least in enumerate(EARLY):
+        if least:
+            pl.when(zi < least)(functools.partial(send_weights, order[place]))
+    for piece in order[len(EARLY) :]:
+        send_weights(piece)
     pair_copy(0).wait_recv()
     mixed = part[tp].astype(F32) + pair_in[0].astype(F32)
     for step in range(1, pairs):
@@ -394,8 +399,18 @@
         piece = row_piece(xi, zj, h)
         return remote(piece, piece, fw_send.at[0], ag_recv.at[zj, h], (x_peer, tp))
 
+    last = outer - 1
+
+    def goes_right(zj):
+        far = jnp.logical_and(zj == 0, zi == last - 1)
+        return jnp.logical_and(zi < last, jnp.logical_not(far) if outer > 2 else True)
+
+    def goes_left(zj):
+        far = jnp.logical_and(zj == last, zi == 1)
+        return jnp.logical_and(zi > 0, jnp.logical_not(far) if outer > 2 else True)
+
     for h in range(SPLITS):
-        @pl.when(zi + 1 < outer)
+        @pl.when(zi < last)
         def _():
             row_right(zi, h).start()
 
@@ -405,14 +420,26 @@
 
         row_across(zi, h).start()
 
-    @pl.loop(1, outer)
-    def _(step):
+    if outer > 2:
+        for h in range(SPLITS):
+            @pl.when(zi == 0)
+            def _():
+                row_copy(zi, h, left_send.at[zi], last * inner + xi).start()
+
+            @pl.when(zi == last)
+            def _():
+                row_copy(zi, h, right_send.at[zi], xi).start()
+
+    for stage in (0, ROW_CUTS):
+        relay(stage)
+
+    def pass_on(step):
         for h in range(SPLITS):
             @pl.when(zi - step >= 0)
             def _():
                 row_arrival(zi - step, h).wait_recv()
 
-                @pl.when(zi + 1 < outer)
+                @pl.when(goes_right(zi - step))
                 def _():
                     row_right(zi - step, h).start()
 
@@ -422,14 +449,21 @@
             def _():
                 row_arrival(zi + step, h).wait_recv()
 
-                @pl.when(zi > 0)
+                @pl.when(goes_left(zi + step))
                 def _():
                     row_left(zi + step, h).start()
 
                 row_across(zi + step, h).start()
 
-    for stage in (*range(ROW_CUTS - 1), *range(ROW_CUTS, ROW_CUTS + EARLY[1])):
+    for stage in range(1, ROW_CUTS - 1):
+        if stage < outer:
+            pass_on(stage)
         relay(stage)
+
+    @pl.loop(ROW_CUTS - 1, outer)
+    def _(step):
+        pass_on(step)
+
     for load in shared_loads:
         load.wait()
     up = dot(normed, s_gu[...])
@@ -442,12 +476,38 @@
     own_rows = lax.broadcasted_iota(jnp.int32, (quarter, length), 0) + tp * quarter
     pick = lax.broadcasted_iota(jnp.int32, (quarter, length), 1) == own_rows
 
+    batch = min(outer, 4)
+    tall = batch * quarter
+    cap = hid_pack.shape[1] // batch
+
+    def token_weights(col, zj, expert_id):
+        line = w_in[zj * inner + col, pl.ds(expert_id, 1)]
+        weight = jnp.sum(jnp.where(pick, line, 0.0), axis=1, keepdims=True)
+        return jnp.broadcast_to(weight, (quarter, LANES))
+
     @pl.loop(0, outer)
     def _(zj):
         for j in range(inner):
-            line = w_in[zj * inner + j, pl.ds(sp, 1)]
-            weight = jnp.sum(jnp.where(pick, line, 0.0), axis=1, keepdims=True)
-            w_rows[j, zj] = jnp.broadcast_to(weight, (quarter, LANES))
+            w_rows[j, zj] = token_weights(j, zj, sp)
+        w_peer[zj] = token_weights(xi, zj, x_peer)
+
+    t_row = lax.broadcasted_iota(jnp.int32, (tall, tall), 0)
+    t_col = lax.broadcasted_iota(jnp.int32, (tall, tall), 1)
+    same = t_row // quarter == t_col // quarter
+    earlier = jnp.where(jnp.logical_and(same, t_col < t_row), 1.0, 0.0).astype(BF16)
+    slot_base = (t_row // quarter * cap).astype(F32)
+
+    def places(weights):
+        chosen = weights > 0.0
+        rank = dot(earlier, jnp.where(chosen, 1.0, 0.0).astype(BF16))
+        hit = jnp.logical_and(chosen, t_col.astype(F32) == rank + slot_base)
+        return jnp.where(hit, 1.0, 0.0).astype(BF16)
+
+    @pl.loop(0, outer // batch)
+    def _(i):
+        group = pl.ds(i * batch, batch)
+        place_out[i] = places(w_rows[other_x, group].reshape(tall, LANES))
+        place_in[i] = places(w_peer[group].reshape(tall, LANES))
 
     for down in (0, 1):
         own = weight_all(tp, down)
@@ -455,11 +515,8 @@
         theirs = weight_all(mate, down)
         remote(theirs, theirs, own_send.at[down], own_recv.at[down], (sp, mate)).wait_recv()
 
-    batch = min(outer, 4)
-    tall = batch * quarter
-
     def gate_up(col, stage):
-        last = stage == ROW_CUTS - 1
+        final = stage == ROW_CUTS - 1
 
         @pl.loop(0, outer // batch)
         def _(i):
@@ -470,7 +527,7 @@
                 gu = dot(block, w_gu[t, stage * depth : (stage + 1) * depth])
                 if stage:
                     gu = gu + gu_acc[col, i, :, t * 2 * fe : (t + 1) * 2 * fe]
-                if last:
+                if final:
                     act = (silu(gu[:, :fe]) * gu[:, fe:]).astype(BF16)
                     hid[col, i, :, t * fe : (t + 1) * fe] = act
                 else:
@@ -479,13 +536,21 @@
     for stage in range(ROW_CUTS - 1):
         from_mate(stage)
         gate_up(xi, stage)
+    relay(ROW_CUTS - 1)
     side = rows.at[other_x]
     remote(side, side, fw_send.at[0], agx_recv.at[0], (x_peer, tp)).wait_recv()
     for stage in range(ROW_CUTS - 1):
         gate_up(other_x, stage)
-    relay(ROW_CUTS - 1)
     from_mate(ROW_CUTS - 1)
     gate_up(other_x, ROW_CUTS - 1)
+
+    @pl.loop(0, outer // batch)
+    def _(i):
+        packed = lax.dot_general(
+            place_out[i], hid[other_x, i], (((0,), (0,)), ((), ())), preferred_element_type=F32
+        )
+        hid_pack[i] = packed[: batch * cap].astype(BF16)
+
     gate_up(xi, ROW_CUTS - 1)
 
     def columns(ref, c):
@@ -503,20 +568,28 @@
             (zj * inner + xi, tp),
         )
 
-    def down(c, col, dest):
+    def down_across(c):
         first, wide = spans[c]
 
         @pl.loop(0, outer // batch)
         def _(i):
             value = dot(
-                hid[col, i], w_d[:, :, first : first + wide].reshape(tp_n * fe, wide)
+                hid_pack[i], w_d[:, :, first : first + wide].reshape(tp_n * fe, wide)
             )
-            weight = w_rows[col, pl.ds(i * batch, batch)].reshape(tall, LANES)
+            y_out[i, :, first : first + wide] = value.astype(BF16)
+
+    def down_own(c):
+        first, wide = spans[c]
+
+        @pl.loop(0, outer // batch)
+        def _(i):
+            value = dot(
+                hid[xi, i], w_d[:, :, first : first + wide].reshape(tp_n * fe, wide)
+            )
+            weight = w_rows[xi, pl.ds(i * batch, batch)].reshape(tall, LANES)
             for a in range(0, wide, LANES):
-                dest[pl.ds(i * batch, batch), :, first + a : first + a + LANES] = (
-                    (weight * value[:, a : a + LANES])
-                    .astype(dest.dtype)
-                    .reshape(batch, quarter, LANES)
+                y_own[pl.ds(i * batch, batch), :, first + a : first + a + LANES] = (
+                    (weight * value[:, a : a + LANES]).reshape(batch, quarter, LANES)
                 )
 
     def merge(c):
@@ -524,27 +597,32 @@
         at = slice(first, first + wide)
         x_out(c).wait_recv()
 
+        @pl.loop(0, outer // batch)
+        def _(i):
+            group = pl.ds(i * batch, batch)
+            value = dot(place_in[i][:, : batch * cap], x_in[i, :, at])
+            weight = w_peer[group].reshape(tall, LANES)
+            for a in range(0, wide, LANES):
+                cols = slice(first + a, first + a + LANES)
+                z_out[group, :, cols] = (
+                    y_own[group, :, cols]
+                    + (weight * value[:, a : a + LANES]).reshape(batch, quarter, LANES)
+                ).astype(BF16)
+
         @pl.loop(1, outer)
         def _(step):
-            zj = lax.rem(zi + step, outer)
-            z_out[zj, :, at] = (
-                y_own[zj, :, at].astype(F32) + x_in[zj, :, at].astype(F32)
-            ).astype(BF16)
             z_send(c, step).start()
 
-        moe[:, at] = moe[:, at] + (y_own[zi, :, at].astype(F32) + x_in[zi, :, at].astype(F32))
+        moe[:, at] = moe[:, at] + z_out[zi, :, at].astype(F32)
 
     chunks = len(spans)
-    ahead = max(EARLY[1], 1)
-    if EARLY[1] == 0:
-        relay(ROW_CUTS)
     for c in range(chunks):
-        if ahead <= c + 1 < chunks:
+        if c + 1 < chunks:
             relay(ROW_CUTS + c + 1)
         from_mate(ROW_CUTS + c)
-        down(c, other_x, y_out)
+        down_across(c)
         x_out(c).start()
-        down(c, xi, y_own)
+        down_own(c)
         if c >= 2:
             merge(c - 2)
     merge(chunks - 2)
@@ -589,11 +667,21 @@
     def _(zj):
         block = rows.at[xi, zj]
 
-        @pl.when(jnp.logical_and(zj <= zi, zi + 1 < outer))
+        ends = jnp.logical_and(zj == zi, outer > 2)
+
+        @pl.when(
+            jnp.logical_or(
+                jnp.logical_and(zj <= zi, goes_right(zj)), jnp.logical_and(ends, zi == last)
+            )
+        )
         def _():
             remote(block, block, right_send.at[zj], fw_send.at[0], (x_peer, tp)).wait_send()
 
-        @pl.when(jnp.logical_and(zj >= zi, zi > 0))
+        @pl.when(
+            jnp.logical_or(
+                jnp.logical_and(zj >= zi, goes_left(zj)), jnp.logical_and(ends, zi == 0)
+            )
+        )
         def _():
             remote(block, block, left_send.at[zj], fw_send.at[0], (x_peer, tp)).wait_send()
 
@@ -642,6 +730,8 @@
     pairs = tp_n // 2
     stages = ROW_CUTS + len(COLUMN_CUTS)
     batch = min(outer, 4)
+    tall = batch * quarter
+    cap = 5 * quarter * routed_expert_index.shape[1] // (4 * sp_n)
     operands = (
         stream,
         recurrence_input,
@@ -685,6 +775,9 @@
             pltpu.VMEM((sp_n, length), F32),
             pltpu.VMEM((sp_n, sp_n, length), F32),
             pltpu.VMEM((inner, outer, quarter, LANES), F32),
+            pltpu.VMEM((outer, quarter, LANES), F32),
+            pltpu.VMEM((outer // batch, tall, LANES), BF16),
+            pltpu.VMEM((outer // batch, tall, LANES), BF16),
             pltpu.VMEM((chans, width), BF16),
             pltpu.VMEM((tp_n, width, 2 * fe), BF16),
             pltpu.VMEM((tp_n, fe, width), BF16),
@@ -695,9 +788,14 @@
             pltpu.VMEM((pairs,) + block, BF16),
             pltpu.VMEM((pairs,) + block, BF16),
             pltpu.VMEM((inner, outer) + block, BF16),
-            pltpu.VMEM((inner, outer // batch, batch * quarter, tp_n * fe), BF16),
+            pltpu.VMEM((inner, outer // batch, tall, tp_n * fe), BF16),
+            pltpu.VMEM((outer // batch, batch * cap, tp_n * fe), BF16),
             pltpu.VMEM((inner, outer // batch, batch * quarter, tp_n * 2 * fe), F32),
-            *(pltpu.VMEM((outer,) + block, BF16) for _ in range(5)),
+            pltpu.VMEM((outer,) + block, F32),
+            pltpu.VMEM((outer // batch, batch * cap, width), BF16),
+            pltpu.VMEM((outer // batch, batch * cap, width), BF16),
+            pltpu.VMEM((outer,) + block, BF16),
+            pltpu.VMEM((outer,) + block, BF16),
             pltpu.VMEM(block, F32),
             dma((6,)),
             dma((2,)),

time: 56.9 us -> 55.4 us (0.974)
  Pallas kernels: 56.1 us -> 54.6 us
    pallas_call x1, Pallas kernels: 56.1 us -> 54.6 us  [shards(): pl.pallas_call(functools.partial(kernel, dims), out_shape=jax.ShapeDtypeS...]
where the time goes in v4:
time: 55.4 us; the launch traced here: 55.3 us
  Pallas kernels  54.6 us (99%)
  local copies, waits for them, and re-layouts  0.66 us (1%)
    pallas_call x1, Pallas kernels, shards(): pl.pallas_call(functools.partial(kernel, dims), out_shape=jax.ShapeDtypeS...  54.6 us

profile of v4, /device:TPU:0, one launch (start us, length us, event | category | flops | bytes accessed | tf_op | source)
XLA Modules:
  0.0 55.3 jit_solution(8043733683677918519)
XLA Ops:
  0.0 54.6 %shard_map.199 = bf16[32,2048]{1,0:T(8,128)(2,1)S(1)} custom-call(bf16[32,2048]{1,0:T(8,128)(2,1)} %stream_hbm.1, bf16[128,2,256]{2,1,0:T(2,128)(2,1)} %rec_hbm.1, bf16[128,2,256]{2,1,0:T(2,128)(2,1)} %gate_hbm.1, bf16[4,2,256]{2,1,0:T(2,128)(2,1)} %taps_hbm.1, bf16[2,4,64,64]{3,2,1,0:T(8,128)(2,1)} %small_hbm.1, bf16[2,2,128,128]{3,2,1,0:T(8,128)(2,1)} %large_hbm.1, ...), custom_call_target="tpu_custom_call" | custom-call | tf_op jit(solution)/shard_map/pallas_call | solution.py:763
  54.6 0.7 %copy.23 = bf16[32,2048]{1,0:T(8,128)(2,1)} copy(bf16[32,2048]{1,0:T(8,128)(2,1)S(1)} %shard_map.199) | data formatting | bytes 262144

commit v5 on v4

--- a/solution.py
+++ b/solution.py
@@ -12,7 +12,7 @@
 LANES = 128
 ROW_CUTS = 4
 COLUMN_CUTS = (2, 2, 2, 2, 2, 2, 2, 2)
-EARLY = (0, 1, 1, 1)
+EARLY = (0, 0, 1, 2)
 SPLITS = 2
 MESH = pl.DeviceIdType.MESH
 F32 = jnp.float32
@@ -79,12 +79,11 @@
     result,
     stream, rec_in, gate_in, taps, small_maps, large_maps, channel_decay, extra, n1g, n1b, n2g, n2b,
     ids, wts, in_sem,
-    padded, halo, carry_own, carry_in, wdense, w_in, w_rows, w_peer, place_out, place_in, out_w, w_gu, w_d, s_gu, s_d,
+    padded, halo, scan_a, scan_b, carry_own, carry_in, wdense, w_in, w_rows, w_peer, place_out, place_in, out_w, w_gu, w_d, s_gu, s_d,
     part, pair_in, pair_out, part_in, rows, hid, hid_pack, gu_acc, y_own, y_out, x_in, z_out, z_in, moe,
     local_sem, halo_sem, carry_send, carry_recv, w_send, w_recv,
     out_send, own_send, relay_send, own_recv, far_recv, relay_recv, pair_send, pair_recv,
-    tp_send, tp_recv, right_send, left_send, fw_send, ag_recv, agx_recv,
-    xs_send, xs_recv, zs_send, zs_recv,
+    tp_send, tp_recv, fw_send, ag_recv, agx_recv, xs_send, zs_send,
 ):
     sp_n, tp_n, inner = dims
     outer = sp_n // inner
@@ -107,6 +106,9 @@
         spans.append((sum(COLUMN_CUTS[:c]) * unit, COLUMN_CUTS[c] * unit))
     half_w = width // SPLITS
 
+    xs_recv, zs_recv = in_sem, carry_recv
+    right_send, left_send = carry_send.at[pl.ds(0, outer)], carry_send.at[pl.ds(outer, outer)]
+
     def remote(src, dst, send, recv, where):
         return pltpu.make_async_remote_copy(
             src_ref=src, dst_ref=dst, send_sem=send, recv_sem=recv,
@@ -212,14 +214,14 @@
         (lax.rem(sp + 1, sp_n), tp),
     )
     pl.semaphore_wait(barrier, sp_n - 1 + tp_n - 1)
-    order = [0, 1, gate_pieces, *range(2, gate_pieces), *range(gate_pieces + 1, len(pieces))]
+    order = [0, gate_pieces, *range(1, gate_pieces), *range(gate_pieces + 1, len(pieces))]
 
     def send_weights(piece):
         for step in range(1, pairs):
             weight_out(piece, step).start()
 
     for place, least in enumerate(EARLY):
-        pl.when(zi >= least)(functools.partial(send_weights, order[place]))
+        pl.when(sp >= least)(functools.partial(send_weights, order[place]))
     loads[0].wait()
 
     @pl.when(sp + 1 < sp_n)
@@ -262,6 +264,37 @@
     ]
 
     padded[pl.ds(8, length)] = rec_in[...].astype(F32).reshape(length, chans)
+    tap_n = taps.shape[0]
+
+    def segment(first, count):
+        base = 8 + first - tap_n + 1
+        summed = tap_rows[0] * padded[pl.ds(base, count)]
+        for k in range(1, tap_n):
+            summed = summed + tap_rows[k] * padded[pl.ds(base + k, count)]
+        conv = summed.astype(BF16)
+        outs = [
+            dot(conv[:, i * LANES : (i + 1) * LANES], maps)
+            for i, maps in enumerate(small_blocks + large_blocks)
+        ]
+        recur = jax.nn.sigmoid(jnp.concatenate([o[:, :LANES] for o in outs], axis=1))
+        inp = jax.nn.sigmoid(jnp.concatenate([o[:, LANES:] for o in outs], axis=1))
+        log_decay = recur * rate + extra[pl.ds(first, count)].reshape(count, chans)
+        decay = jnp.exp(log_decay)
+        state = jnp.sqrt(-expm1_negative(2.0 * log_decay)) * inp * conv.astype(F32)
+        row_id = lax.broadcasted_iota(jnp.int32, (count, chans), 0)
+        shift = 1
+        while shift < count:
+            live = row_id >= shift
+            before_a = jnp.where(live, pltpu.roll(decay, shift, 0), 1.0)
+            before_b = jnp.where(live, pltpu.roll(state, shift, 0), 0.0)
+            state = decay * before_b + state
+            decay = decay * before_a
+            shift *= 2
+        return decay, state
+
+    decay_b, state_b = segment(8, length - 8)
+    scan_a[...] = decay_b
+    scan_b[...] = state_b
 
     @pl.when(sp == 0)
     def _():
@@ -272,31 +305,10 @@
         halo_copy.wait_recv()
         padded[pl.ds(0, 8)] = halo[...].astype(F32).reshape(8, chans)
 
-    tap_n = taps.shape[0]
-    summed = tap_rows[0] * padded[pl.ds(8 - tap_n + 1, length)]
-    for k in range(1, tap_n):
-        summed = summed + tap_rows[k] * padded[pl.ds(8 - tap_n + 1 + k, length)]
-    conv = summed.astype(BF16)
-    outs = [
-        dot(conv[:, i * LANES : (i + 1) * LANES], maps)
-        for i, maps in enumerate(small_blocks + large_blocks)
-    ]
-    recur = jax.nn.sigmoid(jnp.concatenate([o[:, :LANES] for o in outs], axis=1))
-    inp = jax.nn.sigmoid(jnp.concatenate([o[:, LANES:] for o in outs], axis=1))
-    log_decay = recur * rate + extra[...].reshape(length, chans)
-    decay = jnp.exp(log_decay)
-    state = jnp.sqrt(-expm1_negative(2.0 * log_decay)) * inp * conv.astype(F32)
-    row_id = lax.broadcasted_iota(jnp.int32, (length, chans), 0)
-    shift = 1
-    while shift < length:
-        live = row_id >= shift
-        before_a = jnp.where(live, pltpu.roll(decay, shift, 0), 1.0)
-        before_b = jnp.where(live, pltpu.roll(state, shift, 0), 0.0)
-        state = decay * before_b + state
-        decay = decay * before_a
-        shift *= 2
+    decay_a, state_a = segment(0, 8)
+    end_a, end_b = scan_a[length - 9 :], scan_b[length - 9 :]
     carry_own[...] = jnp.concatenate(
-        [decay[length - 1 :], state[length - 1 :]], axis=0
+        [end_a * decay_a[7:], end_a * state_a[7:] + end_b], axis=0
     )
 
     def carry_out(step):
@@ -331,7 +343,9 @@
         return link[0:1] * incoming + link[1:2]
 
     incoming = lax.fori_loop(0, sp, fold, jnp.zeros((1, chans), F32))
-    branch = (gelu * (state + decay * incoming)).astype(BF16)
+    head = state_a + decay_a * incoming
+    rest = scan_b[...] + scan_a[...] * head[7:]
+    branch = (gelu * jnp.concatenate([head, rest], axis=0)).astype(BF16)
     out_w_load.wait()
     part[...] = dot(branch, out_w[...]).astype(BF16).reshape(part.shape)
 
@@ -364,9 +378,15 @@
         part_out(step).start()
     for place, least in enumerate(EARLY):
         if least:
-            pl.when(zi < least)(functools.partial(send_weights, order[place]))
+            pl.when(sp < least)(functools.partial(send_weights, order[place]))
     for piece in order[len(EARLY) :]:
         send_weights(piece)
+    @pl.loop(1, sp_n)
+    def _(step):
+        @pl.when(sp + step < sp_n)
+        def _():
+            carry_out(step).wait_send()
+
     pair_copy(0).wait_recv()
     mixed = part[tp].astype(F32) + pair_in[0].astype(F32)
     for step in range(1, pairs):
@@ -561,8 +581,14 @@
             columns(y_out, c), columns(x_in, c), xs_send.at[0], xs_recv.at[c], (x_peer, tp)
         )
 
+    def z_target(step):
+        down_to, up_to = last + 1 - step, step - 1
+        down_to = jnp.where(down_to > zi, down_to, down_to - 1)
+        up_to = jnp.where(up_to < zi, up_to, up_to + 1)
+        return jnp.where(zi < outer // 2, down_to, up_to)
+
     def z_send(c, step):
-        zj = lax.rem(zi + step, outer)
+        zj = z_target(step)
         return remote(
             columns(z_out, c).at[zj], columns(z_in, c).at[zi], zs_send.at[0], zs_recv.at[c],
             (zj * inner + xi, tp),
@@ -652,12 +678,6 @@
     for step in range(1, pairs):
         part_out(step).wait_send()
     remote(tables, tables, w_send.at[0], w_recv.at[0], (x_peer, tp)).wait_send()
-
-    @pl.loop(1, sp_n)
-    def _(step):
-        @pl.when(sp + step < sp_n)
-        def _():
-            carry_out(step).wait_send()
 
     @pl.when(sp + 1 < sp_n)
     def _():
@@ -770,6 +790,8 @@
             dma((len(operands),)),
             pltpu.VMEM((length + 8, chans), F32),
             pltpu.VMEM((8,) + recurrence_input.shape[1:], BF16),
+            pltpu.VMEM((length - 8, chans), F32),
+            pltpu.VMEM((length - 8, chans), F32),
             pltpu.VMEM((2, chans), F32),
             pltpu.VMEM((sp_n, 2, chans), F32),
             pltpu.VMEM((sp_n, length), F32),
@@ -813,15 +835,11 @@
             dma((pairs,)),
             dma((pairs - 1,)),
             dma((pairs - 1,)),
-            dma((outer,)),
-            dma((outer,)),
             dma((1,)),
             dma((outer, SPLITS)),
             dma((1,)),
             dma((1,)),
-            dma((len(COLUMN_CUTS),)),
             dma((1,)),
-            dma((len(COLUMN_CUTS),)),
         ],
         compiler_params=pltpu.CompilerParams(
             has_side_effects=True, collective_id=0, vmem_limit_bytes=limit

time: 55.4 us -> 55 us (level)
  no operation moved by 1% of the time
where the time goes in v5:
time: 55 us; the launch traced here: 54.9 us
  Pallas kernels  54.2 us (99%)
  local copies, waits for them, and re-layouts  0.66 us (1%)
    pallas_call x1, Pallas kernels, shards(): pl.pallas_call(functools.partial(kernel, dims), out_shape=jax.ShapeDtypeS...  54.2 us

profile of v5, /device:TPU:0, one launch (start us, length us, event | category | flops | bytes accessed | tf_op | source)
XLA Modules:
  0.0 54.9 jit_solution(7925182414171300591)
XLA Ops:
  0.0 54.2 %shard_map.199 = bf16[32,2048]{1,0:T(8,128)(2,1)S(1)} custom-call(bf16[32,2048]{1,0:T(8,128)(2,1)} %stream_hbm.1, bf16[128,2,256]{2,1,0:T(2,128)(2,1)} %rec_hbm.1, bf16[128,2,256]{2,1,0:T(2,128)(2,1)} %gate_hbm.1, bf16[4,2,256]{2,1,0:T(2,128)(2,1)} %taps_hbm.1, bf16[2,4,64,64]{3,2,1,0:T(8,128)(2,1)} %small_hbm.1, bf16[2,2,128,128]{3,2,1,0:T(8,128)(2,1)} %large_hbm.1, ...), custom_call_target="tpu_custom_call" | custom-call | tf_op jit(solution)/shard_map/pallas_call | solution.py:783
  54.2 0.7 %copy.23 = bf16[32,2048]{1,0:T(8,128)(2,1)} copy(bf16[32,2048]{1,0:T(8,128)(2,1)S(1)} %shard_map.199) | data formatting | bytes 262144

commit v6 on v5

--- a/solution.py
+++ b/solution.py
@@ -643,11 +643,11 @@
 
     chunks = len(spans)
     for c in range(chunks):
-        if c + 1 < chunks:
-            relay(ROW_CUTS + c + 1)
         from_mate(ROW_CUTS + c)
         down_across(c)
         x_out(c).start()
+        if c + 1 < chunks:
+            relay(ROW_CUTS + c + 1)
         down_own(c)
         if c >= 2:
             merge(c - 2)

time: 55 us -> 55 us (level)
  no operation moved by 1% of the time
where the time goes in v6:
time: 55 us; the launch traced here: 54.9 us
  Pallas kernels  54.2 us (99%)
  local copies, waits for them, and re-layouts  0.66 us (1%)
    pallas_call x1, Pallas kernels, shards(): pl.pallas_call(functools.partial(kernel, dims), out_shape=jax.ShapeDtypeS...  54.2 us

profile of v6, /device:TPU:0, one launch (start us, length us, event | category | flops | bytes accessed | tf_op | source)
XLA Modules:
  0.0 54.9 jit_solution(15504659143575899707)
XLA Ops:
  0.0 54.2 %shard_map.199 = bf16[32,2048]{1,0:T(8,128)(2,1)S(1)} custom-call(bf16[32,2048]{1,0:T(8,128)(2,1)} %stream_hbm.1, bf16[128,2,256]{2,1,0:T(2,128)(2,1)} %rec_hbm.1, bf16[128,2,256]{2,1,0:T(2,128)(2,1)} %gate_hbm.1, bf16[4,2,256]{2,1,0:T(2,128)(2,1)} %taps_hbm.1, bf16[2,4,64,64]{3,2,1,0:T(8,128)(2,1)} %small_hbm.1, bf16[2,2,128,128]{3,2,1,0:T(8,128)(2,1)} %large_hbm.1, ...), custom_call_target="tpu_custom_call" | custom-call | tf_op jit(solution)/shard_map/pallas_call | solution.py:783
  54.2 0.7 %copy.23 = bf16[32,2048]{1,0:T(8,128)(2,1)} copy(bf16[32,2048]{1,0:T(8,128)(2,1)S(1)} %shard_map.199) | data formatting | bytes 262144
